TPU v7x, 256 devices: a whole 4x4x8 slice. The times are simulated.
256 devices in a mesh: kv: 64 (over z, y, core), tp: 4 (over x).
Axes of the slice: x: 4, y: 4, z: 8, core: 2. Of those that a mesh axis runs over, the one named last changes fastest.
Arguments:
- tokens: bfloat16 [24576, 1024], P('kv', 'tp'), may hold values from -6 to 6
- query_weight: bfloat16 [1024, 512], P(None, 'tp'), may hold values from -0.1875 to 0.1875
- key_weight: bfloat16 [1024, 512], P(None, 'tp'), may hold values from -0.1875 to 0.1875
- value_weight: bfloat16 [1024, 512], P(None, 'tp'), may hold values from -0.1875 to 0.1875
- out_weight: bfloat16 [512, 1024], P('tp'), may hold values from -0.25 to 0.25
- norm_gain: float32 [512], P('tp'), may hold values from 0.1 to 1.9
- chosen_owner: int32 [384, 8], P('kv'), may hold values from 0 to 63, all different within a row; in each aligned block of 6 rows (0 to 5, 6 to 11, ...) at most 1 rows name the same one
- chosen_local: int32 [384, 8], P('kv'), may hold values from 0 to 5
Outputs:
- attended_out: bfloat16 [24576, 1024], P('kv', 'tp')
Inputs may be any that keep to these rules, and one draw needn't show every extreme that they name: `chosen_owner`: each row names 8 different owners; among the 6 rows of one device no owner is named by more than 1 rows, and in some device's rows one owner is named by exactly 1. `chosen_local`: any index of a key block within its owner.
All inputs are finite; a program needn't handle non-finite values.
Results may differ from a plain program's by a relative error of at most 0.015.
Values may be sent and summed in bfloat16 or wider, within the bound.
A program may use at most 64 MiB of HBM per device.

v0:
```python
import jax
import jax.numpy as jnp
from jax import lax
from jax.sharding import PartitionSpec as P

HEADS = 8
HEAD_SIZE = 64
BLOCK = 64


neg_fill = -1e30
eps_norm = 1e-06


def folded(value, axis, dim, take_in, carry):
    whole = jax.tree.map(lambda part: lax.all_gather(part, axis, axis=dim, tiled=True), value)
    return take_in(carry, whole, jnp.int32(0))


def for_sending(value):
    return jax.tree.map(lambda a: a.astype(jnp.bfloat16) if a.dtype == jnp.float32 else a, value)


def scattered(portion, width, axis):
    count = width * lax.axis_size(axis)
    sent = portion(jnp.int32(0), count).astype(jnp.bfloat16)
    return lax.psum_scatter(sent, axis, scatter_dimension=0, tiled=True).astype(jnp.float32)


def partial_softmax(query_rows, key_rows, value_rows, query_pos, key_pos):
    score_scale = query_rows.shape[-1] ** (-0.5)
    scores = (
        jnp.einsum("bqhd,bcthd->bhqct", query_rows, key_rows, preferred_element_type=jnp.float32)
        * score_scale
    )
    visible = key_pos[:, None, None, :, :] <= query_pos[:, None, :, None, None]
    scores = jnp.where(visible, scores, neg_fill)
    highest = jnp.max(scores, axis=(3, 4))
    weights = jnp.where(visible, jnp.exp(scores - highest[:, :, :, None, None]), jnp.float32(0.0))
    mass_sum = jnp.sum(weights, axis=(3, 4))
    blended = jnp.einsum(
        "bhqct,bcthd->bqhd",
        weights,
        value_rows.astype(jnp.float32),
        precision=lax.Precision.DEFAULT,
    )
    return (highest, mass_sum, blended)


def on_device(
    tokens,
    query_weight,
    key_weight,
    value_weight,
    out_weight,
    norm_gain,
    chosen_owner,
    chosen_local,
):
    tok_rows = tokens.shape[0]
    blocks_here = tok_rows // BLOCK
    heads_here = query_weight.shape[1] // HEAD_SIZE
    empty_sum = jnp.zeros((tok_rows, query_weight.shape[1]), jnp.float32)

    def add_columns(carried, portion, offset):
        span_rows = portion.shape[1]
        return tuple(
            (
                partial_sum
                + jnp.dot(
                    portion,
                    lax.dynamic_slice_in_dim(weight, offset, span_rows, 0),
                    preferred_element_type=jnp.float32,
                )
                for partial_sum, weight in zip(carried, (query_weight, key_weight, value_weight))
            )
        )

    projected = folded(tokens, "tp", 1, add_columns, (empty_sum, empty_sum, empty_sum))
    local_queries, local_keys, local_values = [
        summed.astype(jnp.bfloat16).reshape(blocks_here, BLOCK, heads_here, HEAD_SIZE)
        for summed in projected
    ]
    device = lax.axis_index("kv")
    kv_count = lax.axis_size("kv")
    chosen_count = chosen_owner.shape[1]
    capacity = min(blocks_here, max(1, 2 * blocks_here * chosen_count // kv_count))
    offsets = jnp.arange(BLOCK, dtype=jnp.int32)
    own_global = device * blocks_here + jnp.arange(blocks_here, dtype=jnp.int32)
    query_pos = own_global[:, None] * BLOCK + offsets[None, :]
    flat_owner = chosen_owner.reshape(-1)
    one_hot = (flat_owner[:, None] == jnp.arange(kv_count, dtype=jnp.int32)[None, :]).astype(
        jnp.int32
    )
    earlier = jnp.cumsum(one_hot, axis=0) - one_hot
    flat_slot = jnp.sum(earlier * one_hot, axis=1)
    requests = (
        jnp.zeros((kv_count, capacity), jnp.int32)
        .at[flat_owner, flat_slot]
        .set(chosen_local.reshape(-1))
    )
    incoming = lax.all_to_all(requests, "kv", split_axis=0, concat_axis=0, tiled=True)
    key_pack = local_keys[incoming]
    value_pack = local_values[incoming]
    key_back, value_back = (
        lax.all_to_all(for_sending(key_pack), "kv", split_axis=0, concat_axis=0, tiled=True).astype(
            key_pack.dtype
        ),
        lax.all_to_all(
            for_sending(value_pack), "kv", split_axis=0, concat_axis=0, tiled=True
        ).astype(value_pack.dtype),
    )
    chosen_keys = key_back[flat_owner, flat_slot].reshape(
        blocks_here, chosen_count, BLOCK, heads_here, HEAD_SIZE
    )
    chosen_values = value_back[flat_owner, flat_slot].reshape(
        blocks_here, chosen_count, BLOCK, heads_here, HEAD_SIZE
    )
    all_keys = jnp.concatenate([local_keys[:, None], chosen_keys], axis=1)
    all_values = jnp.concatenate([local_values[:, None], chosen_values], axis=1)
    own_kpos = (own_global[:, None] * BLOCK + offsets[None, :])[:, None, :]
    chosen_kpos = jnp.full((blocks_here, chosen_count, BLOCK), -1, jnp.int32)
    key_pos = jnp.concatenate([own_kpos, chosen_kpos], axis=1)
    highest, mass_sum, blended = partial_softmax(
        local_queries, all_keys, all_values, query_pos, key_pos
    )
    attended = blended / jnp.transpose(mass_sum, (0, 2, 1))[..., None]
    attended = attended.astype(jnp.bfloat16).reshape(tok_rows, heads_here * HEAD_SIZE)
    wide_rows = attended.astype(jnp.float32)
    squares = lax.psum(jnp.sum(wide_rows * wide_rows, axis=1), "tp")
    mean_sq = squares / (HEADS * HEAD_SIZE)
    normed = (wide_rows * lax.rsqrt(mean_sq + eps_norm)[:, None] * norm_gain).astype(jnp.bfloat16)
    out_cols = out_weight.shape[1] // lax.axis_size("tp")

    def out_term(offset, count):
        columns = lax.dynamic_slice_in_dim(out_weight, offset, count, 1)
        return jnp.einsum("fc,tf->ct", columns, normed, preferred_element_type=jnp.float32)

    summed = scattered(out_term, out_cols, "tp")
    return summed.T.astype(jnp.bfloat16)


def solution(mesh):
    return jax.shard_map(
        on_device,
        mesh=mesh,
        in_specs=(
            P("kv", "tp"),
            P(None, "tp"),
            P(None, "tp"),
            P(None, "tp"),
            P("tp", None),
            P("tp"),
            P("kv", None),
            P("kv", None),
        ),
        out_specs=P("kv", "tp"),
        check_vma=False,
    )
```

profile of v0, /device:TPU:1, one launch (start us, length us, event | category | flops | bytes accessed | tf_op | source)
XLA Modules:
  0.0 170.8 jit_solution(6048694214814048981)
XLA Ops:
  6.5 0.8 eq.15
  7.3 0.8 reshape.143
  8.2 0.1 reduce_window_sum.11
  8.3 0.2 select_reduce_fusion
  8.4 0.8 reshape.184
  9.2 0.7 scatter_custom_fusion
  10.0 0.7 copy.50
  10.7 13.2 %all-to-all-start = ((s32[64,1,1]{2,1,0:T(1,128)}), s32[64,1,1]{2,1,0:T(1,128)S(1)}, u32[]{:S(2)}, u32[]{:S(2)}) async-start(s32[64,1,1]{2,1,0:T(1,128)} %copy.50), calls=%async_computation | async-start | bytes 65536 | tf_op jit(solution)/shard_map/all_to_all | solution.py:102
  23.8 12.2 %all_gather.3 = bf16[384,1024]{1,0:T(8,128)(2,1)S(1)} all-gather(bf16[384,256]{1,0:T(8,128)(2,1)} %param.8), channel_id=1, replica_groups=mesh['kv'=64,'tp'=4] {'tp'}, dimensions={1}, use_global_device_ids=true | all-gather | bytes 983040 | tf_op jit(solution)/shard_map/all_gather | solution.py:16
  36.0 1.3 convolution_convert_fusion.1
  37.3 0.1 reshape.147
  37.5 1.2 fusion.28
  38.8 1.0 gather_fusion.2
  39.7 1.5 bitcast_bitcast_fusion
  41.3 4.7 %reshape.195 = bf16[64,2,4096]{2,1,0:T(2,128)(2,1)} reshape(bf16[64,1,2,64,64]{4,3,2,1,0:T(8,128)(2,1)} %bitcast_bitcast_fusion) | data formatting | bytes 2097152
  46.0 12.5 %all-to-all-start.2 = ((bf16[64,2,4096]{2,1,0:T(2,128)(2,1)}), bf16[64,2,4096]{2,1,0:T(2,128)(2,1)}, u32[]{:S(2)}, u32[]{:S(2)}) async-start(bf16[64,2,4096]{2,1,0:T(2,128)(2,1)} %reshape.195), calls=%async_computation.2 | async-start | bytes 2097152 | tf_op jit(solution)/shard_map/all_to_all | solution.py:106
  58.5 0.1 broadcast_in_dim_reshape.8
  58.6 0.4 convolution_convert_fusion.3
  59.0 0.1 reshape.142
  59.1 0.1 broadcast_in_dim_reshape.7
  59.3 0.4 convolution_convert_fusion.2
  59.6 0.1 reshape.146
  59.8 0.2 copy.53
  60.0 1.0 gather_fusion
  60.9 1.5 bitcast_bitcast_fusion.1
  62.5 4.7 %reshape.197 = bf16[64,2,4096]{2,1,0:T(2,128)(2,1)} reshape(bf16[64,1,2,64,64]{4,3,2,1,0:T(8,128)(2,1)} %bitcast_bitcast_fusion.1) | data formatting | bytes 2097152
  67.1 19.8 %all-to-all-done.2 = bf16[64,2,4096]{2,1,0:T(2,128)(2,1)} async-done(((bf16[64,2,4096]{2,1,0:T(2,128)(2,1)}), bf16[64,2,4096]{2,1,0:T(2,128)(2,1)}, u32[]{:S(2)}, u32[]{:S(2)}) %all-to-all-start.2) | async-done | bytes 1048608 | tf_op jit(solution)/shard_map/all_to_all | solution.py:106
  86.9 6.5 %all-to-all-start.1 = ((bf16[64,2,4096]{2,1,0:T(2,128)(2,1)}), bf16[64,2,4096]{2,1,0:T(2,128)(2,1)}, u32[]{:S(2)}, u32[]{:S(2)}) async-start(bf16[64,2,4096]{2,1,0:T(2,128)(2,1)} %reshape.197), calls=%async_computation.1 | async-start | bytes 2097152 | tf_op jit(solution)/shard_map/all_to_all | solution.py:109
  93.4 0.2 reduce-scatter.2.cloned.1.call-start
  93.8 0.6 broadcast_compare_fusion
  94.4 3.8 %reshape.196 = bf16[64,1,2,64,64]{4,3,2,1,0:T(8,128)(2,1)S(1)} reshape(bf16[64,2,4096]{2,1,0:T(2,128)(2,1)} %all-to-all-done.2) | data formatting | bytes 2097152
  98.2 2.0 %gather_fusion.3 = bf16[48,64,2,64]{3,1,2,0:T(8,128)(2,1)} fusion(bf16[64,1,64,2,64]{4,2,3,1,0:T(8,128)(2,1)S(1)} %bitcast.58, s32[48]{0:T(128)S(1)} %get-tuple-element.5), kind=kCustom, calls=%fused_computation.3 | custom fusion | bytes 1573248 | tf_op jit(solution)/shard_map/gather | solution.py:113
  100.2 1.9 %pad_maximum_fusion = bf16[6,9,64,2,64]{4,2,1,3,0:T(8,128)(2,1)S(1)} fusion(bf16[6,1,64,2,64]{4,2,1,3,0:T(8,128)(2,1)S(1)} %copy.57, bf16[6,8,64,2,64]{4,2,3,1,0:T(8,128)(2,1)} %bitcast.60), kind=kLoop, calls=%fused_computation.13 | loop fusion | flops 1769472 | bytes 1769472 | tf_op jit(solution)/shard_map/concatenate | solution.py:119
  102.1 0.6 fusion.24
  102.7 0.6 fusion
  103.3 1.1 copy-done.1
  104.5 1.1 fusion.1
  105.5 16.3 %all-to-all-done.1 = bf16[64,2,4096]{2,1,0:T(2,128)(2,1)} async-done(((bf16[64,2,4096]{2,1,0:T(2,128)(2,1)}), bf16[64,2,4096]{2,1,0:T(2,128)(2,1)}, u32[]{:S(2)}, u32[]{:S(2)}) %all-to-all-start.1) | async-done | bytes 1048608 | tf_op jit(solution)/shard_map/all_to_all | solution.py:109
  121.8 3.8 %reshape.198 = bf16[64,1,2,64,64]{4,3,2,1,0:T(8,128)(2,1)S(1)} reshape(bf16[64,2,4096]{2,1,0:T(2,128)(2,1)} %all-to-all-done.1) | data formatting | bytes 2097152
  125.6 2.0 %gather_fusion.1 = bf16[48,64,2,64]{3,1,2,0:T(8,128)(2,1)} fusion(bf16[64,1,64,2,64]{4,2,3,1,0:T(8,128)(2,1)S(1)} %bitcast.59, s32[48]{0:T(128)S(1)} %get-tuple-element.5), kind=kCustom, calls=%fused_computation.1 | custom fusion | bytes 1573248 | tf_op jit(solution)/shard_map/gather | solution.py:116
  127.6 1.9 %copy.54 = bf16[6,8,64,2,64]{2,4,1,3,0:T(8,128)(2,1)S(1)} copy(bf16[6,8,64,2,64]{4,2,3,1,0:T(8,128)(2,1)} %bitcast.61) | data formatting | bytes 1572864 | tf_op jit(solution)/shard_map/reshape | solution.py:116
  129.5 3.8 %multiply_reduce_fusion = (f32[6,64]{1,0:T(8,128)S(1)}, f32[6,64,2,64]{1,3,2,0:T(8,128)S(1)}) fusion(f32[6,64,2]{1,2,0:T(2,128)S(1)} %bitcast.62, f32[6,2,64,9,64]{2,4,3,1,0:T(8,128)} %bitcast.56, f32[6,2,64]{2,1,0:T(2,128)S(1)} %fusion, pred[6,64,9,64]{1,3,2,0:T(8,128)(4,1)S(1)} %broadcast_compare_fusion, bf16[6,8,64,2,64]{2,4,1,3,0:T(8,128)(2,1)S(1)} %copy.54, ...), kind=kOutput, calls=%fused_computation.29 | convolution fusion | flops 59080320 | bytes 3079680 | tf_op jit(solution)/shard_map/bhqct,bcthd->bqhd/dot_general | solution.py:41
  133.3 0.2 copy.61
  133.5 0.2 reshape.149
  133.8 0.1 reduce_sum.35
  133.8 8.8 %psum.7 = f32[384]{0:T(512)S(1)} all-reduce(f32[384]{0:T(512)S(1)} %reduce_sum.35), channel_id=1, replica_groups=mesh['kv'=64,'tp'=4] {'tp'}, use_global_device_ids=true, to_apply=%region_6.7 | all-reduce | flops 384 | bytes 3072 | tf_op jit(solution)/shard_map/psum | solution.py:130
  142.6 1.3 fusion.11
  143.9 20.0 %reduce-scatter.2.cloned.1.call-done = bf16[256,384]{0,1:T(8,128)(2,1)} async-done(((bf16[1024,384]{0,1:T(8,128)(2,1)}), bf16[256,384]{0,1:T(8,128)(2,1)}) %reduce-scatter.2.cloned.1.call-update) | async-done | bytes 196624 | tf_op jit(solution)/shard_map/reduce_scatter | solution.py:27
  (22 shorter events, 0.4 us)
Async XLA Ops:
  6.5 136.1 %copy-start = (bf16[128,1024]{1,0:T(8,128)(2,1)S(1)}, bf16[128,1024]{1,0:T(8,128)(2,1)}, u32[]{:S(2)}) copy-start(bf16[128,1024]{1,0:T(8,128)(2,1)} %param.12) | copy-start | bytes 786436
  10.7 26.8 %all-to-all-start = ((s32[64,1,1]{2,1,0:T(1,128)}), s32[64,1,1]{2,1,0:T(1,128)S(1)}, u32[]{:S(2)}, u32[]{:S(2)}) async-start(s32[64,1,1]{2,1,0:T(1,128)} %copy.50), calls=%async_computation | async-start | bytes 65536 | tf_op jit(solution)/shard_map/all_to_all | solution.py:102
  41.3 17.3 %copy-start.2 = (bf16[1024,128]{1,0:T(8,128)(2,1)S(1)}, bf16[1024,128]{1,0:T(8,128)(2,1)}, u32[]{:S(2)}) copy-start(bf16[1024,128]{1,0:T(8,128)(2,1)} %param.11) | copy-start | bytes 786436
  46.0 13.3 %copy-start.3 = (bf16[1024,128]{1,0:T(8,128)(2,1)S(1)}, bf16[1024,128]{1,0:T(8,128)(2,1)}, u32[]{:S(2)}) copy-start(bf16[1024,128]{1,0:T(8,128)(2,1)} %param.9) | copy-start | bytes 786436
  46.0 41.0 %all-to-all-start.2 = ((bf16[64,2,4096]{2,1,0:T(2,128)(2,1)}), bf16[64,2,4096]{2,1,0:T(2,128)(2,1)}, u32[]{:S(2)}, u32[]{:S(2)}) async-start(bf16[64,2,4096]{2,1,0:T(2,128)(2,1)} %reshape.195), calls=%async_computation.2 | async-start | bytes 2097152 | tf_op jit(solution)/shard_map/all_to_all | solution.py:106
  86.9 34.9 %all-to-all-start.1 = ((bf16[64,2,4096]{2,1,0:T(2,128)(2,1)}), bf16[64,2,4096]{2,1,0:T(2,128)(2,1)}, u32[]{:S(2)}, u32[]{:S(2)}) async-start(bf16[64,2,4096]{2,1,0:T(2,128)(2,1)} %reshape.197), calls=%async_computation.1 | async-start | bytes 2097152 | tf_op jit(solution)/shard_map/all_to_all | solution.py:109
  93.4 70.5 %reduce-scatter.2.cloned.1.call-start = ((), (), s32[]{:S(2)}) async-start(), calls=%async_computation.4 | async-start | bytes 983040 | tf_op jit(solution)/shard_map/reduce_scatter | solution.py:27
  102.7 1.8 %copy-start.1 = (f32[6,2,64,576]{2,3,1,0}, f32[6,2,64,576]{2,3,1,0:S(1)}, u32[]{:S(2)}) copy-start(f32[6,2,64,576]{2,3,1,0:S(1)} %fusion.24) | copy-start | bytes 5308420
  129.5 13.1 %copy-start.4 = (f32[128]{0:T(128)S(1)}, f32[128]{0:T(128)}, u32[]{:S(2)}) copy-start(f32[128]{0:T(128)} %param.13) | copy-start | bytes 1540
Sparse Core Ops, SparseCore 0:
  144.1 19.8 reduce-scatter.1
where the time goes:
time: 173 us; the launch traced here: 171 us
  waiting for transfers between devices  56.1 us (32%)
  local copies, waits for them, and re-layouts  34 us (20%)
  starting transfers between devices  32.3 us (19%)
  blocking collectives  21 us (12%)
  between operations  13.7 us (8%)
  matrix products  7.75 us (4%)
  other arithmetic  5.96 us (3%)
    unnamed x16, local copies, waits for them, and re-layouts  21.1 us
    reduce_scatter x1, waiting for transfers between devices, scattered(): lax.psum_scatter(sent, axis, scatter_dimension=0, tiled=True)  20 us
    all_to_all x1, waiting for transfers between devices, on_device(): lax.all_to_all(for_sending(key_pack), 'kv', split_axis=0, concat_axis=0,...  19.8 us
    all_to_all x1, waiting for transfers between devices, on_device(): lax.all_to_all(for_sending(value_pack), 'kv', split_axis=0, concat_axis=0...  16.3 us
    all_to_all x1, starting transfers between devices, on_device(): lax.all_to_all(requests, 'kv', split_axis=0, concat_axis=0, tiled=True)  13.2 us
    all_to_all x1, starting transfers between devices, on_device(): lax.all_to_all(for_sending(key_pack), 'kv', split_axis=0, concat_axis=0,...  12.5 us
    all_gather x1, blocking collectives, folded(): lax.all_gather(part, axis, axis=dim, tiled=True)  12.2 us
    psum x1, blocking collectives, on_device(): squares = lax.psum(jnp.sum(wide_rows * wide_rows, axis=1), 'tp')  8.75 us
  transfers between devices with their start and end apart: 4, of which 3 were waited for; matrix products, arithmetic and copies ran while one was open for 12% of the time, Pallas kernels for 0%

commit v1 on v0

v1 whole, which is shorter than its diff:
```python
import jax
import jax.numpy as jnp
from jax import lax
from jax.experimental import pallas as pl
from jax.experimental.pallas import tpu as pltpu
from jax.sharding import PartitionSpec as P

MESH = pl.DeviceIdType.MESH
BF16, F32, I32 = jnp.bfloat16, jnp.float32, jnp.int32

HEADS = 8
HEAD_SIZE = 64
BLOCK = 64
CHOSEN = 8
NB = 6
FEATS = 128
PART = 256
NZ, NY, NX = 8, 4, 4
NEG = -1e30
EPS = 1e-06
CH = 3
VMEM, SMEM, DMA = pltpu.VMEM, pltpu.SMEM, pltpu.SemaphoreType.DMA

NT = (((1,), (1,)), ((), ()))
NN = (((1,), (0,)), ((), ()))


def dot(a, b, dims=NN):
    return lax.dot_general(a, b, dims, preferred_element_type=F32)


def sems(**shapes):
    found = {}
    for name, shape in shapes.items():
        found["s_" + name] = DMA(shape)
        found["r_" + name] = DMA(shape)
    return found


def place():
    kv, x = lax.axis_index("kv"), lax.axis_index("tp")
    return lax.rem(kv, 2), lax.rem(lax.div(kv, 2), NY), lax.div(kv, 2 * NY), x


def device(dz=0, dy=0, dx=0, flip=False):
    c, y, z, x = place()
    zz, yy, xx = lax.rem(z + dz, NZ), lax.rem(y + dy, NY), lax.rem(x + dx, NX)
    return ((zz * NY + yy) * 2 + (1 - c if flip else c), xx)


def sender(r):
    def send(src, dst, name, index, to):
        return pltpu.make_async_remote_copy(
            src_ref=src,
            dst_ref=dst,
            send_sem=r["s_" + name].at[index],
            recv_sem=r["r_" + name].at[index],
            device_id=to,
            device_id_type=MESH,
        )

    return send


def greet(peers):
    barrier = pltpu.get_barrier_semaphore()
    for peer in peers:
        pl.semaphore_signal(barrier, inc=1, device_id=peer, device_id_type=MESH)
    return lambda: pl.semaphore_wait(barrier, len(peers))


def rows_of(i, n=BLOCK):
    return pl.ds(i * n, n)


def masks():
    lane = lax.broadcasted_iota(I32, (BLOCK, FEATS), 1)
    sub = lax.broadcasted_iota(I32, (BLOCK, FEATS), 0)
    low = (lane < HEAD_SIZE).astype(F32).astype(BF16)
    high = (lane >= HEAD_SIZE).astype(F32).astype(BF16)
    pick = (lax.rem(lane, HEAD_SIZE) == sub).astype(F32).astype(BF16)
    visible = sub <= lax.rem(lane, HEAD_SIZE)

    def spread(a):
        return jnp.concatenate([a * low, a * high], axis=0)

    return spread, pick, visible


def project_scratch():
    shapes = {f"tok{j}": VMEM((NB * BLOCK, PART), BF16) for j in range(4)}
    shapes["w"] = VMEM((1024, 3 * FEATS), BF16)
    shapes["s_in"] = DMA((4,))
    return shapes | sems(x=(3, NB))


def project(tok_hbm, wq_hbm, wk_hbm, wv_hbm, kv_ref, q_ref, *refs):
    r = dict(zip(project_scratch(), refs))
    x = lax.axis_index("tp")
    send = sender(r)
    ins = [pltpu.make_async_copy(tok_hbm, r["tok0"], r["s_in"].at[0])]
    for n, ref in enumerate((wk_hbm, wv_hbm, wq_hbm)):
        ins.append(pltpu.make_async_copy(ref, r["w"].at[:, pl.ds(n * FEATS, FEATS)], r["s_in"].at[n + 1]))
    for copy in ins:
        copy.start()
    greeted = greet([device(dx=j) for j in (1, 2, 3)])
    spread, pick, _ = masks()
    ins[0].wait()
    greeted()

    def x_own(kind, i):
        dst, dx = ("tok1", 1) if kind == 0 else ("tok3", 3)
        return send(r["tok0"].at[rows_of(i)], r[dst].at[rows_of(i)], "x", (kind, i), device(dx=dx))

    def x_far(i):
        src, dx = ("tok1", 1) if i % 2 == 0 else ("tok3", 3)
        return send(r[src].at[rows_of(i)], r["tok2"].at[rows_of(i)], "x", (2, i), device(dx=dx))

    for i in (0, 1):
        x_own(0, i).start()
        x_own(1, i).start()
    for copy in ins[1:]:
        copy.wait()

    def block(i):
        x_far(i).wait_recv()
        total = jnp.zeros((BLOCK, 3 * FEATS), F32)
        for j in range(4):
            part = pl.ds(pl.multiple_of(lax.rem(x + NX - j, NX) * PART, PART), PART)
            total = total + dot(r[f"tok{j}"][rows_of(i), :], r["w"][part, :])
        kv_ref[i, 0] = total[:, :FEATS].astype(BF16)
        kv_ref[i, 1] = dot(pick, spread(total[:, FEATS : 2 * FEATS].astype(BF16)), NT).astype(BF16)
        q_ref[i] = total[:, 2 * FEATS :].astype(BF16)

    for i in range(NB):
        x_own(0, i).wait_recv()
        x_own(1, i).wait_recv()
        x_far(i).start()
        if i + 2 < NB:
            x_own(0, i + 2).start()
            x_own(1, i + 2).start()
        if i >= 1:
            block(i - 1)
    block(NB - 1)
    for i in range(NB):
        x_own(0, i).wait_send()
        x_own(1, i).wait_send()
        x_far(i).wait_send()


def attend_scratch():
    shapes = {}
    for j in range(4):
        shapes[f"codes{j}"] = VMEM((8, 128), I32)
        if j:
            shapes[f"q{j}"] = VMEM((NB, BLOCK, FEATS), BF16)
    for dz in range(-3, 5):
        if dz:
            shapes[f"kv{dz}"] = VMEM((NB, 2, BLOCK, FEATS), BF16)
        shapes[f"other{dz}"] = VMEM((NB, 2, BLOCK, FEATS), BF16)
    shapes["codes_s"] = SMEM((4, 8, 128), I32)
    for name in ("p", "r"):
        shapes[name + "o"] = VMEM((3, NB, BLOCK, FEATS), BF16)
        shapes[name + "m"] = VMEM((3, NB, 8, FEATS), F32)
    shapes["item_o"] = VMEM((4, 2 * NZ, BLOCK, FEATS), F32)
    shapes["item_m"] = VMEM((4, 2 * NZ, 8, FEATS), F32)
    shapes["own_o"] = VMEM((NB, BLOCK, FEATS), F32)
    shapes["own_m"] = VMEM((NB, 8, FEATS), F32)
    shapes["s_codes"] = DMA((4,))
    return shapes | sems(z=(2, 4, NB), p=(8,), y=(4,), c=(4,), b=(4, CH), m=(4, CH))


def attend_all(kv_ref, q_ref, owner_ref, local_ref, out_ref, *refs):
    r = dict(zip(attend_scratch(), refs))
    r["kv0"], r["q0"] = kv_ref, q_ref
    c, y, z, x = place()
    send = sender(r)
    peers = [device(dy=j) for j in (1, 2, 3)] + [device(dz=1), device(dz=NZ - 1), device(flip=True)]
    greeted = greet(peers)

    lane8 = lax.broadcasted_iota(I32, (8, 128), 1)
    row8 = lax.broadcasted_iota(I32, (8, 128), 0)
    by_owner = jnp.zeros((8, 128), I32)
    listed = jnp.zeros((8, 128), I32)
    for row in range(NB):
        for ch in range(CHOSEN):
            owner = owner_ref[row, ch]
            by_owner = jnp.where(lane8 == owner, row * 8 + local_ref[row, ch], by_owner)
            listed = jnp.where(lane8 == row * 8 + ch, owner, listed)
    r["codes0"][...] = jnp.where(row8 == 0, by_owner, listed)
    spread, pick, visible = masks()
    greeted()

    def z_has(d, k, i):
        return k < 4 or (k == 4 and (i < NB // 2) == (d == 0))

    def z_copy(d, k, i):
        sign = -1 if d == 0 else 1
        src, dst = sign * (k - 1), (4 if k == 4 else sign * k)
        return send(
            r[f"kv{src}"].at[i], r[f"kv{dst}"].at[i], "z", (d, k - 1, i), device(dz=1 if d == 0 else NZ - 1)
        )

    def z_event(k, i):
        for d in (0, 1):
            if z_has(d, k, i):
                z_copy(d, k, i).wait_recv()
                if z_has(d, k + 1, i):
                    z_copy(d, k + 1, i).start()
        if i == NB - 1:
            for dz in (-k, k) if k < 4 else (4,):
                pair(dz).start()

    def pair(dz):
        return send(r[f"kv{dz}"], r[f"other{dz}"], "p", dz + 3, device(flip=True))

    def y_query(j):
        return send(r["q0"], r[f"q{j}"], "y", j, device(dy=j))

    def y_codes(j):
        return send(r["codes0"], r[f"codes{j}"], "c", j, device(dy=j))

    def y_back(j, t):
        two = pl.ds(2 * t, 2)
        to = device(dy=NY - j)
        return (
            send(r["po"].at[j - 1, two], r["ro"].at[j - 1, two], "b", (j, t), to),
            send(r["pm"].at[j - 1, two], r["rm"].at[j - 1, two], "m", (j, t), to),
        )

    for i in range(NB):
        for d in (0, 1):
            z_copy(d, 1, i).start()
    for j in (2, 1, 3):
        y_codes(j).start()
        y_query(j).start()
    pair(0).start()

    def attend(q, k, v_t, causal=False):
        scores = dot(k, spread(q), NT) * (HEAD_SIZE**-0.5)
        if causal:
            scores = jnp.where(visible, scores, NEG)
        highest = jnp.max(scores, axis=0, keepdims=True)
        weights = jnp.exp(scores - highest)
        if causal:
            weights = jnp.where(visible, weights, 0.0)
        mass = jnp.sum(weights, axis=0, keepdims=True)
        return highest, mass, dot(v_t, spread(weights.astype(BF16)))

    def own(b, _=None):
        highest, mass, blended = attend(r["q0"][b], r["kv0"][b, 0], r["kv0"][b, 1], causal=True)
        r["own_m"][b, 0:1] = highest
        r["own_m"][b, 1:2] = mass
        r["own_o"][b] = blended

    lax.fori_loop(0, NB, own, None)
    for i in range(NB):
        z_event(1, i)
        if i == 2:
            for j in (1, 2, 3):
                y_codes(j).wait_recv()
            tables = [
                pltpu.make_async_copy(r[f"codes{j}"], r["codes_s"].at[j], r["s_codes"].at[j]) for j in range(4)
            ]
            for copy in tables:
                copy.start()
        if i == 4:
            for copy in tables:
                copy.wait()
    for j in (1, 2, 3):
        y_query(j).wait_recv()

    def group(dz, flip):
        if flip:
            pair(dz).wait_recv()
        ref = r[f"other{dz}" if flip else f"kv{dz}"]
        side = 1 - c if flip else c
        zz = lax.rem(z + dz + NZ, NZ)
        owner, slot = (zz * NY + y) * 2 + side, zz * 2 + side

        def items(_, __):
            for j in range(4):
                code = r["codes_s"][j, 0, owner]
                row, loc = lax.div(code, 8), lax.rem(code, 8)
                highest, mass, blended = attend(r[f"q{j}"][row], ref[loc, 0], ref[loc, 1])
                r["item_m"][j, slot, 0:1] = highest
                r["item_m"][j, slot, 1:2] = mass
                r["item_o"][j, slot] = blended

        lax.fori_loop(0, 1, items, None)

    groups = [(0, False), (0, True)]
    for k in (1, 2, 3):
        groups += [(-k, False), (k, False), (-k, True), (k, True)]
    groups += [(4, False), (4, True)]
    for i in range(NB):
        z_event(2, i)
        group(*groups[i])
    for i in range(NB):
        z_event(3, i)
        if i < 4:
            group(*groups[6 + i])
    for i in range(NB):
        z_event(4, i)
        if i % 2 == 0:
            group(*groups[10 + i // 2])
    for g in groups[13:]:
        group(*g)

    def merged(j, b, mine=False):
        parts = []
        for ch in range(CHOSEN):
            owner = r["codes_s"][j, 1, b * 8 + ch]
            ok = lax.rem(lax.div(owner, 2), NY) == y
            slot = lax.div(owner, 2 * NY) * 2 + lax.rem(owner, 2)
            here = jnp.broadcast_to(ok.astype(I32), (1, FEATS)) > 0
            parts.append((here, r["item_m"][j, slot, 0:1], r["item_m"][j, slot, 1:2], r["item_o"][j, slot]))
        if mine:
            yes = jnp.full((1, FEATS), True)
            parts.append((yes, r["own_m"][b, 0:1], r["own_m"][b, 1:2], r["own_o"][b]))
        tops = [jnp.where(here, m, NEG) for here, m, _, _ in parts]
        top = tops[0]
        for m in tops[1:]:
            top = jnp.maximum(top, m)
        mass = jnp.zeros((1, FEATS), F32)
        blended = jnp.zeros((BLOCK, FEATS), F32)
        for (here, _, l, o), m in zip(parts, tops):
            scale = jnp.where(here, jnp.exp(m - top), 0.0)
            mass = mass + scale * l
            blended = blended + scale * o
        return top, mass, blended

    def back(step, _):
        t, j = lax.div(step, 3), 1 + lax.rem(step, 3)
        for n in range(2):
            b = 2 * t + n
            top, mass, blended = merged(j, b)
            r["pm"][j - 1, b, 0:1] = top
            r["pm"][j - 1, b, 1:2] = mass
            r["po"][j - 1, b] = blended.astype(BF16)
        for copy in y_back(j, t):
            copy.start()

    lax.fori_loop(0, 3 * CH, back, None)

    def finish(t, _):
        held = [merged(0, 2 * t + n, mine=True) for n in range(2)]
        for j in (1, 2, 3):
            for copy in y_back(j, t):
                copy.wait_recv()
        for n in range(2):
            b = 2 * t + n
            parts = [held[n]] + [
                (r["rm"][j, b, 0:1], r["rm"][j, b, 1:2], r["ro"][j, b].astype(F32)) for j in range(3)
            ]
            top = parts[0][0]
            for m, _, _ in parts[1:]:
                top = jnp.maximum(top, m)
            mass = jnp.zeros((1, FEATS), F32)
            blended = jnp.zeros((BLOCK, FEATS), F32)
            for m, l, o in parts:
                scale = jnp.exp(m - top)
                mass = mass + scale * l
                blended = blended + scale * o
            attended = (blended / mass).astype(BF16)
            out_ref[pl.ds(b * BLOCK, BLOCK), :] = dot(pick, spread(attended), NT).astype(BF16)

    lax.fori_loop(0, CH, finish, None)

    for i in range(NB):
        for d in (0, 1):
            for k in (1, 2, 3, 4):
                if z_has(d, k, i):
                    z_copy(d, k, i).wait_send()
    for dz in range(-3, 5):
        pair(dz).wait_send()
    for j in (1, 2, 3):
        y_codes(j).wait_send()
        y_query(j).wait_send()
        for t in range(CH):
            for copy in y_back(j, t):
                copy.wait_send()


def close_scratch():
    shapes = {}
    for j in range(4):
        shapes[f"gain{j}"] = VMEM((8, FEATS), F32)
        if j:
            shapes[f"att{j}"] = VMEM((NB * BLOCK, FEATS), BF16)
    return shapes | sems(g=(4,), a=(4, CH))


def close(att_ref, wo0_ref, wo1_ref, wo2_ref, wo3_ref, gain_ref, out_ref, *refs):
    r = dict(zip(close_scratch(), refs))
    r["att0"] = att_ref
    wo = (wo0_ref, wo1_ref, wo2_ref, wo3_ref)
    send = sender(r)
    greeted = greet([device(dx=j) for j in (1, 2, 3)])
    r["gain0"][...] = jnp.broadcast_to(gain_ref[...], (8, FEATS))
    greeted()

    def x_gain(j):
        return send(r["gain0"], r[f"gain{j}"], "g", j, device(dx=j))

    def x_att(j, t):
        rows = rows_of(t, 2 * BLOCK)
        return send(r["att0"].at[rows], r[f"att{j}"].at[rows], "a", (j, t), device(dx=j))

    for j in (2, 1, 3):
        x_gain(j).start()
    for t in range(CH):
        for j in (2, 1, 3):
            x_att(j, t).start()
    for j in (1, 2, 3):
        x_gain(j).wait_recv()
    for t in range(CH):
        for j in (1, 2, 3):
            x_att(j, t).wait_recv()
        rows = rows_of(t, 2 * BLOCK)
        wide = [r[f"att{j}"][rows, :].astype(F32) for j in range(4)]
        squares = sum(jnp.sum(a * a, axis=1, keepdims=True) for a in wide)
        scale = lax.rsqrt(squares / (HEADS * HEAD_SIZE) + EPS)
        total = jnp.zeros((2 * BLOCK, PART), F32)
        for j in range(4):
            normed = (wide[j] * scale * r[f"gain{j}"][0:1, :]).astype(BF16)
            total = total + dot(normed, wo[j][...])
        out_ref[rows, :] = total.astype(BF16)

    for j in (1, 2, 3):
        x_gain(j).wait_send()
        for t in range(CH):
            x_att(j, t).wait_send()


def call(body, name, shapes, specs, outs, collective, flops, operands):
    vmem = pl.BlockSpec(memory_space=VMEM)
    return pl.pallas_call(
        body,
        out_shape=outs,
        in_specs=specs,
        out_specs=jax.tree.map(lambda _: vmem, outs),
        scratch_shapes=list(shapes.values()),
        compiler_params=pltpu.CompilerParams(
            collective_id=collective, has_side_effects=True, vmem_limit_bytes=24 * 2**20
        ),
        cost_estimate=pl.CostEstimate(flops=flops, bytes_accessed=2**20, transcendentals=0),
        name=name,
    )(*operands)


def on_device(tokens, query_weight, key_weight, value_weight, out_weight, norm_gain, chosen_owner, chosen_local):
    hbm = pl.BlockSpec(memory_space=pltpu.HBM)
    vmem = pl.BlockSpec(memory_space=VMEM)
    smem = pl.BlockSpec(memory_space=SMEM)
    x = lax.axis_index("tp")
    columns = [lax.dynamic_slice_in_dim(out_weight, lax.rem(x + j, NX) * PART, PART, 1) for j in range(NX)]
    shifted = columns[:1] + [
        lax.ppermute(columns[j], "tp", [(i, (i + j) % NX) for i in range(NX)]) for j in range(1, NX)
    ]
    keys_values = jax.ShapeDtypeStruct((NB, 2, BLOCK, FEATS), BF16)
    queries = jax.ShapeDtypeStruct((NB, BLOCK, FEATS), BF16)
    rows = NB * BLOCK
    kv, q = call(
        project, "project", project_scratch(), [hbm] * 4, (keys_values, queries), 0, 10**9,
        (tokens, query_weight, key_weight, value_weight),
    )
    att = call(
        attend_all, "attend", attend_scratch(), [vmem, vmem, smem, smem], jax.ShapeDtypeStruct((rows, FEATS), BF16),
        1, 10**10, (kv, q, chosen_owner, chosen_local),
    )
    return call(
        close, "close", close_scratch(), [vmem] * 6, jax.ShapeDtypeStruct((rows, PART), BF16), 2, 10**9,
        (att, *shifted, norm_gain.reshape(1, FEATS)),
    )


def solution(mesh):
    return jax.shard_map(
        on_device,
        mesh=mesh,
        in_specs=(
            P("kv", "tp"),
            P(None, "tp"),
            P(None, "tp"),
            P(None, "tp"),
            P("tp", None),
            P("tp"),
            P("kv", None),
            P("kv", None),
        ),
        out_specs=P("kv", "tp"),
        check_vma=False,
    )
```

time: 173 us -> 76.6 us (0.44); the launches traced: 171 us -> 76.4 us
  Pallas kernels: 0 us -> 66.4 us
  waiting for transfers between devices: 56.1 us -> 0.01 us
  local copies, waits for them, and re-layouts: 34 us -> 4.23 us
  starting transfers between devices: 32.3 us -> 5.72 us
  blocking collectives: 21 us -> 0 us
  between operations: 13.7 us -> 0.08 us
  matrix products: 7.75 us -> 0 us
  other arithmetic: 5.96 us -> 0 us
    pallas_call x0 -> x3, Pallas kernels: none -> 66.4 us  [call(): pl.pallas_call(body, out_shape=outs, in_specs=specs, out_specs=jax.tree.m...]
    all_to_all x3 -> x0, waiting for transfers between devices: 36.1 us -> none  [the longest x1 19.8 us: on_device(): lax.all_to_all(for_sending(key_pack), 'kv', split_axis=0, concat_axis=0,...]
    all_to_all x3 -> x0, starting transfers between devices: 32.1 us -> none  [the longest x1 13.2 us: on_device(): lax.all_to_all(requests, 'kv', split_axis=0, concat_axis=0, tiled=True)]
    reduce_scatter x1 -> x0, waiting for transfers between devices: 20 us -> none  [scattered(): lax.psum_scatter(sent, axis, scatter_dimension=0, tiled=True)]
    unnamed x16 -> x15, local copies, waits for them, and re-layouts: 21.1 us -> 3.22 us
    all_gather x1 -> x0, blocking collectives: 12.2 us -> none  [folded(): lax.all_gather(part, axis, axis=dim, tiled=True)]
    psum x1 -> x0, blocking collectives: 8.75 us -> none  [on_device(): squares = lax.psum(jnp.sum(wide_rows * wide_rows, axis=1), 'tp')]
    dot_general x5 -> x0, matrix products: 7.15 us -> none  [the longest x1 3.8 us: partial_softmax(): jnp.einsum('bhqct,bcthd->bqhd', weights, value_rows.astype(jnp.float32),...]
  transfers between devices with their start and end apart: 4 -> 3, of which waited for: 3 -> 0; matrix products, arithmetic and copies ran while one was open for 12% -> 0% of each run, Pallas kernels for 0% -> 76%
where the time goes in v1:
time: 76.6 us; the launch traced here: 76.4 us
  Pallas kernels  66.4 us (87%)
  starting transfers between devices  5.72 us (7%)
  local copies, waits for them, and re-layouts  4.23 us (6%)
    pallas_call x3, Pallas kernels, call(): pl.pallas_call(body, out_shape=outs, in_specs=specs, out_specs=jax.tree.m...  66.4 us
    ppermute x3, starting transfers between devices, on_device(): lax.ppermute(columns[j], 'tp', [(i, (i + j) % NX) for i in range(NX)])  5.72 us
    unnamed x15, local copies, waits for them, and re-layouts  3.22 us
  transfers between devices with their start and end apart: 3, of which 0 were waited for; matrix products, arithmetic and copies ran while one was open for 0% of the time, Pallas kernels for 76%

profile of v1, /device:TPU:1, one launch (start us, length us, event | category | flops | bytes accessed | tf_op | source)
XLA Modules:
  0.0 76.4 jit_solution(11465204292029066445)
XLA Ops:
  0.0 0.0 copy-start
  0.0 0.0 copy-start.1
  0.0 1.0 %constant_dynamic-slice_fusion = (bf16[128,256]{1,0:T(8,128)(2,1)S(1)}, bf16[128,256]{1,0:T(8,128)(2,1)S(1)}, bf16[128,256]{1,0:T(8,128)(2,1)S(1)}, bf16[128,256]{1,0:T(8,128)(2,1)S(1)}) fusion(bf16[128,1024]{1,0:T(8,128)(2,1)} %param.12, s32[]{:T(128)S(6)} %select_n.15, s32[]{:T(128)S(6)} %select_n.13, s32[]{:T(128)S(6)} %select_n.12, s32[]{:T(128)S(6)} %select_n.14), kind=kLoop, calls=%fused_computation | loop fusion | bytes 524304 | tf_op jit(solution)/shard_map/dynamic_slice | solution.py:457
  1.0 2.1 %collective-permute-start = (bf16[128,256]{1,0:T(8,128)(2,1)S(1)}, bf16[128,256]{1,0:T(8,128)(2,1)S(1)}, u32[]{:S(2)}, u32[]{:S(2)}) collective-permute-start(bf16[128,256]{1,0:T(8,128)(2,1)S(1)} %get-tuple-element.10), channel_id=1, source_target_pairs={{0,1},{1,2},{2,3},{3,0},{4,5},{5,6},{6,7},{7,4},{8,9},{9,10},{10,1... | collective-permute-start | bytes 196616 | tf_op jit(solution)/shard_map/ppermute | solution.py:459
  3.1 2.5 %collective-permute-start.1 = (bf16[128,256]{1,0:T(8,128)(2,1)S(1)}, bf16[128,256]{1,0:T(8,128)(2,1)S(1)}, u32[]{:S(2)}, u32[]{:S(2)}) collective-permute-start(bf16[128,256]{1,0:T(8,128)(2,1)S(1)} %get-tuple-element.12), channel_id=1, source_target_pairs={{0,2},{1,3},{2,0},{3,1},{4,6},{5,7},{6,4},{7,5},{8,10},{9,11},{10,... | collective-permute-start | bytes 196616 | tf_op jit(solution)/shard_map/ppermute | solution.py:459
  5.6 1.2 %collective-permute-start.2 = (bf16[128,256]{1,0:T(8,128)(2,1)S(1)}, bf16[128,256]{1,0:T(8,128)(2,1)S(1)}, u32[]{:S(2)}, u32[]{:S(2)}) collective-permute-start(bf16[128,256]{1,0:T(8,128)(2,1)S(1)} %get-tuple-element.9), channel_id=1, source_target_pairs={{0,3},{1,0},{2,1},{3,2},{4,7},{5,4},{6,5},{7,6},{8,11},{9,8},{10,9... | collective-permute-start | bytes 196616 | tf_op jit(solution)/shard_map/ppermute | solution.py:459
  6.7 0.0 copy-done
  6.7 0.0 copy-done.1
  6.7 0.0 copy-start.2
  6.7 0.9 %copy-done.2 = bf16[1024,128]{1,0:T(8,128)(2,1)S(1)} copy-done((bf16[1024,128]{1,0:T(8,128)(2,1)S(1)}, bf16[1024,128]{1,0:T(8,128)(2,1)}, u32[]{:S(2)}) %copy-start.2) | copy-done | bytes 262168
  7.7 0.0 copy-start.3
  7.7 0.9 %copy-done.3 = bf16[384,256]{1,0:T(8,128)(2,1)S(1)} copy-done((bf16[384,256]{1,0:T(8,128)(2,1)S(1)}, bf16[384,256]{1,0:T(8,128)(2,1)}, u32[]{:S(2)}) %copy-start.3) | copy-done | bytes 196632
  8.6 0.0 copy-start.4
  8.6 0.0 copy-start.5
  8.6 14.8 %project.1 = (bf16[6,2,64,128]{3,2,1,0:T(8,128)(2,1)S(1)}, bf16[6,64,128]{2,1,0:T(8,128)(2,1)S(1)}) custom-call(bf16[384,256]{1,0:T(8,128)(2,1)S(1)} %copy-done.3, bf16[1024,128]{1,0:T(8,128)(2,1)S(1)} %copy-done, bf16[1024,128]{1,0:T(8,128)(2,1)S(1)} %copy-done.1, bf16[1024,128]{1,0:T(8,128)(2,1)S(1)} %copy-done.2), custom_call_target="tpu_custom_call" | custom-call | flops 1000000000 | bytes 1048576 | tf_op jit(solution)/shard_map/project/pallas_call | solution.py:438
  23.4 0.0 copy-done.4
  23.4 0.0 copy-done.5
  23.4 43.1 %attend.1.att_ref = bf16[384,128]{1,0:T(8,128)(2,1)S(1)} custom-call(bf16[6,2,64,128]{3,2,1,0:T(8,128)(2,1)S(1)} %get-tuple-element.7.kv_ref, bf16[6,64,128]{2,1,0:T(8,128)(2,1)S(1)} %get-tuple-element.8.q_ref, s32[6,8]{1,0:T(8,128)S(1)} %copy-done.4, s32[6,8]{1,0:T(8,128)S(1)} %copy-done.5), custom_call_target="tpu_custom_call" | custom-call | flops 10000000000 | bytes 1048576 | tf_op jit(solution)/shard_map/attend/pallas_call | solution.py:438
  66.5 0.0 collective-permute-done.wo1_ref
  66.5 0.0 collective-permute-done.1.wo2_ref
  66.5 0.0 collective-permute-done.2.wo3_ref
  66.6 0.0 copy-start.6
  66.6 0.6 copy-done.6
  67.2 8.5 %close.1 = bf16[384,256]{1,0:T(8,128)(2,1)S(1)} custom-call(bf16[384,128]{1,0:T(8,128)(2,1)S(1)} %attend.1.att_ref, bf16[128,256]{1,0:T(8,128)(2,1)S(1)} %get-tuple-element.11.wo0_ref, bf16[128,256]{1,0:T(8,128)(2,1)S(1)} %collective-permute-done.wo1_ref, bf16[128,256]{1,0:T(8,128)(2,1)S(1)} %collective-permute-done.1.wo2_ref, ...), custom_call_target="tpu_custom_call" | custom-call | flops 1000000000 | bytes 1048576 | tf_op jit(solution)/shard_map/close/pallas_call | solution.py:438
  75.7 0.7 copy.10
Async XLA Ops:
  0.0 6.7 %copy-start = (bf16[1024,128]{1,0:T(8,128)(2,1)S(1)}, bf16[1024,128]{1,0:T(8,128)(2,1)}, u32[]{:S(2)}) copy-start(bf16[1024,128]{1,0:T(8,128)(2,1)} %wq_hbm.1) | copy-start | bytes 786436
  0.0 6.7 %copy-start.1 = (bf16[1024,128]{1,0:T(8,128)(2,1)S(1)}, bf16[1024,128]{1,0:T(8,128)(2,1)}, u32[]{:S(2)}) copy-start(bf16[1024,128]{1,0:T(8,128)(2,1)} %wk_hbm.1) | copy-start | bytes 786436
  1.0 65.5 %collective-permute-start = (bf16[128,256]{1,0:T(8,128)(2,1)S(1)}, bf16[128,256]{1,0:T(8,128)(2,1)S(1)}, u32[]{:S(2)}, u32[]{:S(2)}) collective-permute-start(bf16[128,256]{1,0:T(8,128)(2,1)S(1)} %get-tuple-element.10), channel_id=1, source_target_pairs={{0,1},{1,2},{2,3},{3,0},{4,5},{5,6},{6,7},{7,4},{8,9},{9,10},{10,1... | collective-permute-start | bytes 196616 | tf_op jit(solution)/shard_map/ppermute | solution.py:459
  3.1 63.4 %collective-permute-start.1 = (bf16[128,256]{1,0:T(8,128)(2,1)S(1)}, bf16[128,256]{1,0:T(8,128)(2,1)S(1)}, u32[]{:S(2)}, u32[]{:S(2)}) collective-permute-start(bf16[128,256]{1,0:T(8,128)(2,1)S(1)} %get-tuple-element.12), channel_id=1, source_target_pairs={{0,2},{1,3},{2,0},{3,1},{4,6},{5,7},{6,4},{7,5},{8,10},{9,11},{10,... | collective-permute-start | bytes 196616 | tf_op jit(solution)/shard_map/ppermute | solution.py:459
  5.6 61.0 %collective-permute-start.2 = (bf16[128,256]{1,0:T(8,128)(2,1)S(1)}, bf16[128,256]{1,0:T(8,128)(2,1)S(1)}, u32[]{:S(2)}, u32[]{:S(2)}) collective-permute-start(bf16[128,256]{1,0:T(8,128)(2,1)S(1)} %get-tuple-element.9), channel_id=1, source_target_pairs={{0,3},{1,0},{2,1},{3,2},{4,7},{5,4},{6,5},{7,6},{8,11},{9,8},{10,9... | collective-permute-start | bytes 196616 | tf_op jit(solution)/shard_map/ppermute | solution.py:459
  6.7 1.0 %copy-start.2 = (bf16[1024,128]{1,0:T(8,128)(2,1)S(1)}, bf16[1024,128]{1,0:T(8,128)(2,1)}, u32[]{:S(2)}) copy-start(bf16[1024,128]{1,0:T(8,128)(2,1)} %wv_hbm.1) | copy-start | bytes 786436
  7.7 0.9 %copy-start.3 = (bf16[384,256]{1,0:T(8,128)(2,1)S(1)}, bf16[384,256]{1,0:T(8,128)(2,1)}, u32[]{:S(2)}) copy-start(bf16[384,256]{1,0:T(8,128)(2,1)} %tok_hbm.1) | copy-start | bytes 589828
  8.6 14.8 %copy-start.4 = (s32[6,8]{1,0:T(8,128)S(1)}, s32[6,8]{1,0:T(8,128)}, u32[]{:S(2)}) copy-start(s32[6,8]{1,0:T(8,128)} %owner_ref.1) | copy-start | bytes 580
  8.6 14.8 %copy-start.5 = (s32[6,8]{1,0:T(8,128)S(1)}, s32[6,8]{1,0:T(8,128)}, u32[]{:S(2)}) copy-start(s32[6,8]{1,0:T(8,128)} %local_ref.1) | copy-start | bytes 580
  66.6 0.7 copy-start.6

commit v2 on v1

v2 whole, which is shorter than its diff:
```python
import jax
import jax.numpy as jnp
from jax import lax
from jax.experimental import pallas as pl
from jax.experimental.pallas import tpu as pltpu
from jax.sharding import PartitionSpec as P

MESH = pl.DeviceIdType.MESH
BF16, F32, I32 = jnp.bfloat16, jnp.float32, jnp.int32

HEADS = 8
HEAD_SIZE = 64
BLOCK = 64
CHOSEN = 8
NB = 6
FEATS = 128
PART = 256
NZ, NY, NX = 8, 4, 4
NEG = -1e30
EPS = 1e-06
CH = 3

NT = (((1,), (1,)), ((), ()))
NN = (((1,), (0,)), ((), ()))


def dot(a, b, dims=NN):
    return lax.dot_general(a, b, dims, preferred_element_type=F32)


def scratch():
    shapes = {}
    for j in range(4):
        shapes[f"tok{j}"] = pltpu.VMEM((NB * BLOCK, PART), BF16)
        shapes[f"wo{j}"] = pltpu.VMEM((FEATS, PART), BF16)
        shapes[f"gain{j}"] = pltpu.VMEM((8, FEATS), F32)
        shapes[f"q{j}"] = pltpu.VMEM((NB, BLOCK, FEATS), BF16)
        shapes[f"codes{j}"] = pltpu.VMEM((8, 128), I32)
        shapes[f"att{j}"] = pltpu.VMEM((NB * BLOCK, FEATS), BF16)
    for dz in range(-3, 5):
        shapes[f"kv{dz}"] = pltpu.VMEM((NB, 2, BLOCK, FEATS), BF16)
        shapes[f"other{dz}"] = pltpu.VMEM((NB, 2, BLOCK, FEATS), BF16)
    shapes["w"] = pltpu.VMEM((1024, 3 * FEATS), BF16)
    shapes["wo"] = pltpu.VMEM((FEATS, 1024), BF16)
    shapes["codes_s"] = pltpu.SMEM((4, 8, 128), I32)
    for name in ("p", "r"):
        shapes[name + "o"] = pltpu.VMEM((3, NB, BLOCK, FEATS), BF16)
        shapes[name + "m"] = pltpu.VMEM((3, NB, 8, FEATS), F32)
    shapes["item_o"] = pltpu.VMEM((4, 2 * NZ, BLOCK, FEATS), F32)
    shapes["item_m"] = pltpu.VMEM((4, 2 * NZ, 8, FEATS), F32)
    shapes["own_o"] = pltpu.VMEM((NB, BLOCK, FEATS), F32)
    shapes["own_m"] = pltpu.VMEM((NB, 8, FEATS), F32)
    dma = pltpu.SemaphoreType.DMA
    shapes["s_in"] = dma((5,))
    shapes["s_codes"] = dma((4,))
    for name, shape in dict(
        x=(3, NB), z=(2, 4, NB), p=(8,), y=(4, NB), c=(4,), w=(4,), g=(4,), b=(4, CH), m=(4, CH), a=(4, CH)
    ).items():
        shapes["s_" + name] = dma(shape)
        shapes["r_" + name] = dma(shape)
    return shapes


def kernel(tok_hbm, wq_hbm, wk_hbm, wv_hbm, wo_hbm, gain_ref, owner_ref, local_ref, out_ref, *refs):
    r = dict(zip(scratch().keys(), refs))
    kv, x = lax.axis_index("kv"), lax.axis_index("tp")
    c, y, z = lax.rem(kv, 2), lax.rem(lax.div(kv, 2), NY), lax.div(kv, 2 * NY)

    def at(dz=0, dy=0, dx=0, flip=False):
        zz, yy, xx = lax.rem(z + dz, NZ), lax.rem(y + dy, NY), lax.rem(x + dx, NX)
        return ((zz * NY + yy) * 2 + (1 - c if flip else c), xx)

    def send(src, dst, name, index, device):
        return pltpu.make_async_remote_copy(
            src_ref=src,
            dst_ref=dst,
            send_sem=r["s_" + name].at[index],
            recv_sem=r["r_" + name].at[index],
            device_id=device,
            device_id_type=MESH,
        )

    ins = [pltpu.make_async_copy(tok_hbm, r["tok0"], r["s_in"].at[0])]
    for n, ref in enumerate((wk_hbm, wv_hbm, wq_hbm)):
        ins.append(pltpu.make_async_copy(ref, r["w"].at[:, pl.ds(n * FEATS, FEATS)], r["s_in"].at[n + 1]))
    ins.append(pltpu.make_async_copy(wo_hbm, r["wo"], r["s_in"].at[4]))
    for copy in ins:
        copy.start()

    barrier = pltpu.get_barrier_semaphore()
    peers = [at(dx=j) for j in (1, 2, 3)] + [at(dy=j) for j in (1, 2, 3)] + [at(dz=1), at(dz=NZ - 1), at(flip=True)]
    for peer in peers:
        pl.semaphore_signal(barrier, inc=1, device_id=peer, device_id_type=MESH)

    lane8 = lax.broadcasted_iota(I32, (8, 128), 1)
    row8 = lax.broadcasted_iota(I32, (8, 128), 0)
    by_owner = jnp.zeros((8, 128), I32)
    listed = jnp.zeros((8, 128), I32)
    for row in range(NB):
        for ch in range(CHOSEN):
            owner = owner_ref[row, ch]
            by_owner = jnp.where(lane8 == owner, row * 8 + local_ref[row, ch], by_owner)
            listed = jnp.where(lane8 == row * 8 + ch, owner, listed)
    r["codes0"][...] = jnp.where(row8 == 0, by_owner, listed)
    r["gain0"][...] = jnp.broadcast_to(gain_ref[...], (8, FEATS))

    lane = lax.broadcasted_iota(I32, (BLOCK, FEATS), 1)
    sub = lax.broadcasted_iota(I32, (BLOCK, FEATS), 0)
    low = (lane < HEAD_SIZE).astype(F32).astype(BF16)
    high = (lane >= HEAD_SIZE).astype(F32).astype(BF16)
    pick = (lax.rem(lane, HEAD_SIZE) == sub).astype(F32).astype(BF16)

    def spread(a):
        return jnp.concatenate([a * low, a * high], axis=0)

    ins[0].wait()
    pl.semaphore_wait(barrier, len(peers))

    def rows_of(i, n=BLOCK):
        return pl.ds(i * n, n)

    def x_own(kind, i):
        return send(
            r["tok0"].at[rows_of(i)], r["tok1" if kind == 0 else "tok3"].at[rows_of(i)], "x", (kind, i), at(dx=1 if kind == 0 else 3)
        )

    def x_far(i):
        src, dx = ("tok1", 1) if i % 2 == 0 else ("tok3", 3)
        return send(r[src].at[rows_of(i)], r["tok2"].at[rows_of(i)], "x", (2, i), at(dx=dx))

    def z_has(d, k, i):
        return k < 4 or (k == 4 and (i < NB // 2) == (d == 0))

    def z_copy(d, k, i):
        sign = -1 if d == 0 else 1
        src, dst = sign * (k - 1), (4 if k == 4 else sign * k)
        return send(
            r[f"kv{src}"].at[i], r[f"kv{dst}"].at[i], "z", (d, k - 1, i), at(dz=1 if d == 0 else NZ - 1)
        )

    def z_event(k, i):
        for d in (0, 1):
            if z_has(d, k, i):
                z_copy(d, k, i).wait_recv()
                if z_has(d, k + 1, i):
                    z_copy(d, k + 1, i).start()
        if i == NB - 1:
            for dz in (-k, k) if k < 4 else (4,):
                pair(dz).start()

    def pair(dz):
        return send(r[f"kv{dz}"], r[f"other{dz}"], "p", dz + 3, at(flip=True))

    def y_query(j, i):
        return send(r["q0"].at[i], r[f"q{j}"].at[i], "y", (j, i), at(dy=j))

    def y_codes(j):
        return send(r["codes0"], r[f"codes{j}"], "c", j, at(dy=j))

    def x_wo(j):
        cols = pl.ds(pl.multiple_of(lax.rem(x + j, NX) * PART, PART), PART)
        return send(r["wo"].at[:, cols], r[f"wo{j}"], "w", j, at(dx=j))

    def x_gain(j):
        return send(r["gain0"], r[f"gain{j}"], "g", j, at(dx=j))

    def y_back(j, t):
        two = pl.ds(2 * t, 2)
        to = at(dy=NY - j)
        return (
            send(r["po"].at[j - 1, two], r["ro"].at[j - 1, two], "b", (j, t), to),
            send(r["pm"].at[j - 1, two], r["rm"].at[j - 1, two], "m", (j, t), to),
        )

    def x_att(j, t):
        rows = rows_of(t, 2 * BLOCK)
        return send(r["att0"].at[rows], r[f"att{j}"].at[rows], "a", (j, t), at(dx=j))

    sent = []

    def start(copy):
        copy.start()
        sent.append(copy)

    for i in (0, 1):
        x_own(0, i).start()
        x_own(1, i).start()
    for j in (2, 1, 3):
        y_codes(j).start()
    for copy in ins[1:4]:
        copy.wait()

    def project(i):
        x_far(i).wait_recv()

        def block(_, __):
            total = jnp.zeros((BLOCK, 3 * FEATS), F32)
            for j in range(4):
                part = pl.ds(pl.multiple_of(lax.rem(x + NX - j, NX) * PART, PART), PART)
                total = total + dot(r[f"tok{j}"][rows_of(i), :], r["w"][part, :])
            r["kv0"][i, 0] = total[:, :FEATS].astype(BF16)
            r["kv0"][i, 1] = dot(pick, spread(total[:, FEATS : 2 * FEATS].astype(BF16)), NT).astype(BF16)
            r["q0"][i] = total[:, 2 * FEATS :].astype(BF16)

        lax.fori_loop(0, 1, block, None)
        for d in (0, 1):
            z_copy(d, 1, i).start()
        for j in (2, 1, 3):
            y_query(j, i).start()

    for i in range(NB):
        x_own(0, i).wait_recv()
        x_own(1, i).wait_recv()
        x_far(i).start()
        if i + 2 < NB:
            x_own(0, i + 2).start()
            x_own(1, i + 2).start()
        if i >= 1:
            project(i - 1)
        if i >= 4:
            z_event(1, i - 4)
    project(NB - 1)
    pair(0).start()
    ins[4].wait()
    for j in (2, 1, 3):
        x_wo(j).start()
        x_gain(j).start()
    mine = pl.ds(pl.multiple_of(x * PART, PART), PART)
    r["wo0"][...] = r["wo"][:, mine]
    z_event(1, 2)

    def attend(q, k, v_t, causal=False):
        scores = dot(k, spread(q), NT) * (HEAD_SIZE**-0.5)
        if causal:
            visible = sub <= lax.rem(lane, HEAD_SIZE)
            scores = jnp.where(visible, scores, NEG)
        highest = jnp.max(scores, axis=0, keepdims=True)
        weights = jnp.exp(scores - highest)
        if causal:
            weights = jnp.where(visible, weights, 0.0)
        mass = jnp.sum(weights, axis=0, keepdims=True)
        return highest, mass, dot(v_t, spread(weights.astype(BF16)))

    def own(b, _=None):
        highest, mass, blended = attend(r["q0"][b], r["kv0"][b, 0], r["kv0"][b, 1], causal=True)
        r["own_m"][b, 0:1] = highest
        r["own_m"][b, 1:2] = mass
        r["own_o"][b] = blended

    lax.fori_loop(0, NB, own, None)
    z_event(1, 3)
    for j in (1, 2, 3):
        y_codes(j).wait_recv()
    tables = [pltpu.make_async_copy(r[f"codes{j}"], r["codes_s"].at[j], r["s_codes"].at[j]) for j in range(4)]
    for copy in tables:
        copy.start()
    z_event(1, 4)
    z_event(1, 5)
    for copy in tables:
        copy.wait()
    for i in range(NB):
        for j in (1, 2, 3):
            y_query(j, i).wait_recv()

    def group(dz, flip):
        if flip:
            pair(dz).wait_recv()
        ref = r[f"other{dz}" if flip else f"kv{dz}"]
        side = 1 - c if flip else c
        zz = lax.rem(z + dz + NZ, NZ)
        owner, slot = (zz * NY + y) * 2 + side, zz * 2 + side

        def items(_, __):
            for j in range(4):
                code = r["codes_s"][j, 0, owner]
                row, loc = lax.div(code, 8), lax.rem(code, 8)
                highest, mass, blended = attend(r[f"q{j}"][row], ref[loc, 0], ref[loc, 1])
                r["item_m"][j, slot, 0:1] = highest
                r["item_m"][j, slot, 1:2] = mass
                r["item_o"][j, slot] = blended

        lax.fori_loop(0, 1, items, None)

    groups = [(0, False), (0, True)]
    for k in (1, 2, 3):
        groups += [(-k, False), (k, False), (-k, True), (k, True)]
    groups += [(4, False), (4, True)]
    for i in range(NB):
        z_event(2, i)
        group(*groups[i])
    for i in range(NB):
        z_event(3, i)
        if i < 4:
            group(*groups[6 + i])
    for i in range(NB):
        z_event(4, i)
        if i % 2 == 0:
            group(*groups[10 + i // 2])
    for g in groups[13:]:
        group(*g)

    def merged(j, b, mine=False):
        parts = []
        for ch in range(CHOSEN):
            owner = r["codes_s"][j, 1, b * 8 + ch]
            ok = lax.rem(lax.div(owner, 2), NY) == y
            slot = lax.div(owner, 2 * NY) * 2 + lax.rem(owner, 2)
            here = jnp.broadcast_to(ok.astype(I32), (1, FEATS)) > 0
            parts.append((here, r["item_m"][j, slot, 0:1], r["item_m"][j, slot, 1:2], r["item_o"][j, slot]))
        if mine:
            yes = jnp.full((1, FEATS), True)
            parts.append((yes, r["own_m"][b, 0:1], r["own_m"][b, 1:2], r["own_o"][b]))
        tops = [jnp.where(here, m, NEG) for here, m, _, _ in parts]
        top = tops[0]
        for m in tops[1:]:
            top = jnp.maximum(top, m)
        mass = jnp.zeros((1, FEATS), F32)
        blended = jnp.zeros((BLOCK, FEATS), F32)
        for (here, _, l, o), m in zip(parts, tops):
            scale = jnp.where(here, jnp.exp(m - top), 0.0)
            mass = mass + scale * l
            blended = blended + scale * o
        return top, mass, blended

    def back(step, _):
        t, j = lax.div(step, 3), 1 + lax.rem(step, 3)
        for n in range(2):
            b = 2 * t + n
            top, mass, blended = merged(j, b)
            r["pm"][j - 1, b, 0:1] = top
            r["pm"][j - 1, b, 1:2] = mass
            r["po"][j - 1, b] = blended.astype(BF16)
        for copy in y_back(j, t):
            copy.start()

    lax.fori_loop(0, 3 * CH, back, None)

    def finish(t, _):
        held = [merged(0, 2 * t + n, mine=True) for n in range(2)]
        for j in (1, 2, 3):
            for copy in y_back(j, t):
                copy.wait_recv()
        for n in range(2):
            b = 2 * t + n
            parts = [held[n]] + [
                (r["rm"][j, b, 0:1], r["rm"][j, b, 1:2], r["ro"][j, b].astype(F32)) for j in range(3)
            ]
            top = parts[0][0]
            for m, _, _ in parts[1:]:
                top = jnp.maximum(top, m)
            mass = jnp.zeros((1, FEATS), F32)
            blended = jnp.zeros((BLOCK, FEATS), F32)
            for m, l, o in parts:
                scale = jnp.exp(m - top)
                mass = mass + scale * l
                blended = blended + scale * o
            attended = (blended / mass).astype(BF16)
            r["att0"][rows_of(b), :] = dot(pick, spread(attended), NT).astype(BF16)
        for j in (2, 1, 3):
            x_att(j, t).start()

    lax.fori_loop(0, CH, finish, None)

    for j in (1, 2, 3):
        x_wo(j).wait_recv()
        x_gain(j).wait_recv()
    def close(t, _):
        for j in (1, 2, 3):
            x_att(j, t).wait_recv()
        rows = rows_of(t, 2 * BLOCK)
        wide = [r[f"att{j}"][rows, :].astype(F32) for j in range(4)]
        squares = sum(jnp.sum(a * a, axis=1, keepdims=True) for a in wide)
        scale = lax.rsqrt(squares / (HEADS * HEAD_SIZE) + EPS)
        total = jnp.zeros((2 * BLOCK, PART), F32)
        for j in range(4):
            normed = (wide[j] * scale * r[f"gain{j}"][0:1, :]).astype(BF16)
            total = total + dot(normed, r[f"wo{j}"][...])
        out_ref[rows, :] = total.astype(BF16)

    lax.fori_loop(0, CH, close, None)

    for i in range(NB):
        x_own(0, i).wait_send()
        x_own(1, i).wait_send()
        x_far(i).wait_send()
        for j in (1, 2, 3):
            y_query(j, i).wait_send()
        for d in (0, 1):
            for k in (1, 2, 3, 4):
                if z_has(d, k, i):
                    z_copy(d, k, i).wait_send()
    for dz in range(-3, 5):
        pair(dz).wait_send()
    for j in (1, 2, 3):
        y_codes(j).wait_send()
        x_wo(j).wait_send()
        x_gain(j).wait_send()
        for t in range(CH):
            for copy in y_back(j, t):
                copy.wait_send()
            x_att(j, t).wait_send()


def on_device(tokens, query_weight, key_weight, value_weight, out_weight, norm_gain, chosen_owner, chosen_local):
    hbm = pl.BlockSpec(memory_space=pltpu.HBM)
    vmem = pl.BlockSpec(memory_space=pltpu.VMEM)
    smem = pl.BlockSpec(memory_space=pltpu.SMEM)
    return pl.pallas_call(
        kernel,
        out_shape=jax.ShapeDtypeStruct((NB * BLOCK, PART), BF16),
        in_specs=[hbm] * 5 + [vmem, smem, smem],
        out_specs=vmem,
        scratch_shapes=list(scratch().values()),
        compiler_params=pltpu.CompilerParams(collective_id=0, has_side_effects=True),
        name="attend",
    )(tokens, query_weight, key_weight, value_weight, out_weight, norm_gain.reshape(1, FEATS), chosen_owner, chosen_local)


def solution(mesh):
    return jax.shard_map(
        on_device,
        mesh=mesh,
        in_specs=(
            P("kv", "tp"),
            P(None, "tp"),
            P(None, "tp"),
            P(None, "tp"),
            P("tp", None),
            P("tp"),
            P("kv", None),
            P("kv", None),
        ),
        out_specs=P("kv", "tp"),
        check_vma=False,
    )
```

time: 76.6 us -> 62.3 us (0.81)
  Pallas kernels: 66.4 us -> 60.5 us
  starting transfers between devices: 5.72 us -> 0 us
  local copies, waits for them, and re-layouts: 4.23 us -> 1.62 us
    pallas_call x3 -> x1, Pallas kernels: 66.4 us -> 60.5 us  [on_device(): pl.pallas_call(kernel, out_shape=jax.ShapeDtypeStruct((NB * BLOCK, PART),...]
    ppermute x3 -> x0, starting transfers between devices: 5.72 us -> none  [on_device(): lax.ppermute(columns[j], 'tp', [(i, (i + j) % NX) for i in range(NX)])]
    unnamed x15 -> x1, local copies, waits for them, and re-layouts: 3.22 us -> 1.62 us
    dynamic_slice x1 -> x0, local copies, waits for them, and re-layouts: 1.01 us -> none  [on_device(): lax.dynamic_slice_in_dim(out_weight, lax.rem(x + j, NX) * PART, PART, 1)]
  transfers between devices with their start and end apart: 3 -> 0, of which waited for: 0 -> 0; matrix products, arithmetic and copies ran while one was open for 0% -> 0% of each run, Pallas kernels for 76% -> 0%
where the time goes in v2:
time: 62.3 us; the launch traced here: 62.2 us
  Pallas kernels  60.5 us (97%)
  local copies, waits for them, and re-layouts  1.62 us (3%)
    pallas_call x1, Pallas kernels, on_device(): pl.pallas_call(kernel, out_shape=jax.ShapeDtypeStruct((NB * BLOCK, PART),...  60.5 us
    unnamed x1, local copies, waits for them, and re-layouts  1.62 us

profile of v2, /device:TPU:1, one launch (start us, length us, event | category | flops | bytes accessed | tf_op | source)
XLA Modules:
  0.0 62.2 jit_solution(13191808393682861181)
XLA Ops:
  0.0 60.5 %attend.1 = bf16[384,256]{1,0:T(8,128)(2,1)} custom-call(bf16[384,256]{1,0:T(8,128)(2,1)} %tok_hbm.1, bf16[1024,128]{1,0:T(8,128)(2,1)} %wq_hbm.1, bf16[1024,128]{1,0:T(8,128)(2,1)} %wk_hbm.1, bf16[1024,128]{1,0:T(8,128)(2,1)} %wv_hbm.1, bf16[128,1024]{1,0:T(8,128)(2,1)} %wo_hbm.1, f32[1,128]{1,0:T(1,128)} %bitcast.1, s32[6,8]{1,0:T(8,128)} %owner_ref.1, ...), custom_call_target="tpu_custom_call" | custom-call | tf_op jit(solution)/shard_map/attend/pallas_call | solution.py:408
  60.6 1.6 %copy.10 = bf16[384,256]{1,0:T(8,128)(2,1)} copy(bf16[384,256]{1,0:T(8,128)(2,1)} %attend.1) | data formatting | bytes 393216

commit v3 on v2

v3 whole, which is shorter than its diff:
```python
import jax
import jax.numpy as jnp
from jax import lax
from jax.experimental import pallas as pl
from jax.experimental.pallas import tpu as pltpu
from jax.sharding import PartitionSpec as P

MESH = pl.DeviceIdType.MESH
BF16, F32, I32 = jnp.bfloat16, jnp.float32, jnp.int32

HEADS = 8
HEAD_SIZE = 64
BLOCK = 64
CHOSEN = 8
NB = 6
FEATS = 128
PART = 256
NZ, NY, NX = 8, 4, 4
NEG = -1e30
EPS = 1e-06
ASKED = 64
AHEAD = 3
DIRECT = (0, NB - 1)
CH = 3

NT = (((1,), (1,)), ((), ()))
NN = (((1,), (0,)), ((), ()))


def dot(a, b, dims=NN):
    return lax.dot_general(a, b, dims, preferred_element_type=F32)


def scratch():
    shapes = {}
    for j in range(4):
        shapes[f"tok{j}"] = pltpu.VMEM((NB * BLOCK, PART), BF16)
        shapes[f"wo{j}"] = pltpu.VMEM((FEATS, PART), BF16)
        shapes[f"gain{j}"] = pltpu.VMEM((8, FEATS), F32)
        shapes[f"q{j}"] = pltpu.VMEM((NB, BLOCK, FEATS), BF16)
        shapes[f"codes{j}"] = pltpu.VMEM((8, 128), I32)
        shapes[f"att{j}"] = pltpu.VMEM((NB * BLOCK, FEATS), BF16)
    for dz in range(-3, 5):
        shapes[f"kv{dz}"] = pltpu.VMEM((NB, 2, BLOCK, FEATS), BF16)
        shapes[f"other{dz}"] = pltpu.VMEM((NB, 2, BLOCK, FEATS), BF16)
    shapes["w"] = pltpu.VMEM((1024, 3 * FEATS), BF16)
    shapes["wo"] = pltpu.VMEM((FEATS, 1024), BF16)
    shapes["codes_s"] = pltpu.SMEM((4, 8, 128), I32)
    for name in ("p", "r"):
        shapes[name + "o"] = pltpu.VMEM((3, NB, BLOCK, FEATS), BF16)
        shapes[name + "m"] = pltpu.VMEM((3, CH, 8, FEATS), F32)
    for name in ("l", "e"):
        shapes[name + "o"] = pltpu.VMEM((3, 2, BLOCK, FEATS), BF16)
        shapes[name + "m"] = pltpu.VMEM((3, 8, FEATS), F32)
    shapes["item_o"] = pltpu.VMEM((4, 2 * NZ, BLOCK, FEATS), F32)
    shapes["item_m"] = pltpu.VMEM((4, 2 * NZ, 8, FEATS), F32)
    shapes["own_o"] = pltpu.VMEM((NB, BLOCK, FEATS), F32)
    shapes["own_m"] = pltpu.VMEM((NB, 8, FEATS), F32)
    dma = pltpu.SemaphoreType.DMA
    shapes["s_in"] = dma((5,))
    shapes["s_codes"] = dma((4,))
    for name, many, one in (
        ("x", (3, NB), (3,)),
        ("z", (2, 3, NB), (2, 3)),
        ("l", (NB,), (2,)),
        ("p", (8,), (8,)),
        ("y", (3,), (3,)),
        ("c", (3,), (3,)),
        ("w", (3,), (3,)),
        ("g", (3,), (3,)),
        ("b", (3,), (3,)),
        ("m", (3,), (3,)),
        ("e", (3,), (3,)),
        ("f", (3,), (3,)),
        ("a", (3, CH), (3,)),
    ):
        shapes["r_" + name] = dma(many)
        shapes["s_" + name] = dma(one)
    return shapes


def kernel(tok_hbm, wq_hbm, wk_hbm, wv_hbm, wo_hbm, gain_ref, owner_ref, local_ref, out_ref, *refs):
    r = dict(zip(scratch().keys(), refs))
    kv, x = lax.axis_index("kv"), lax.axis_index("tp")
    c, y, z = lax.rem(kv, 2), lax.rem(lax.div(kv, 2), NY), lax.div(kv, 2 * NY)

    def at(dz=0, dy=0, dx=0, flip=False):
        zz, yy, xx = lax.rem(z + dz, NZ), lax.rem(y + dy, NY), lax.rem(x + dx, NX)
        return ((zz * NY + yy) * 2 + (1 - c if flip else c), xx)

    def send(src, dst, name, group, index, device):
        return pltpu.make_async_remote_copy(
            src_ref=src,
            dst_ref=dst,
            send_sem=r["s_" + name].at[group],
            recv_sem=r["r_" + name].at[index],
            device_id=device,
            device_id_type=MESH,
        )

    ins = [pltpu.make_async_copy(tok_hbm, r["tok0"], r["s_in"].at[0])]
    for n, ref in enumerate((wk_hbm, wv_hbm, wq_hbm)):
        ins.append(pltpu.make_async_copy(ref, r["w"].at[:, pl.ds(n * FEATS, FEATS)], r["s_in"].at[n + 1]))
    ins.append(pltpu.make_async_copy(wo_hbm, r["wo"], r["s_in"].at[4]))
    for copy in ins:
        copy.start()

    barrier = pltpu.get_barrier_semaphore()
    peers = [at(dx=j) for j in (1, 2, 3)] + [at(dy=j) for j in (1, 2, 3)] + [at(dz=1), at(dz=NZ - 1), at(flip=True)]
    for peer in peers:
        pl.semaphore_signal(barrier, inc=1, device_id=peer, device_id_type=MESH)

    lane8 = lax.broadcasted_iota(I32, (8, 128), 1)
    row8 = lax.broadcasted_iota(I32, (8, 128), 0)
    by_owner = jnp.zeros((8, 128), I32)
    listed = jnp.zeros((8, 128), I32)
    for row in range(NB):
        for ch in range(CHOSEN):
            owner = owner_ref[row, ch]
            by_owner = jnp.where(lane8 == owner, ASKED + row * 8 + local_ref[row, ch], by_owner)
            listed = jnp.where(lane8 == row * 8 + ch, owner, listed)
    r["codes0"][...] = jnp.where(row8 == 0, by_owner, listed)
    r["gain0"][...] = jnp.broadcast_to(gain_ref[...], (8, FEATS))

    lane = lax.broadcasted_iota(I32, (BLOCK, FEATS), 1)
    sub = lax.broadcasted_iota(I32, (BLOCK, FEATS), 0)
    low = (lane < HEAD_SIZE).astype(F32).astype(BF16)
    high = (lane >= HEAD_SIZE).astype(F32).astype(BF16)
    pick = (lax.rem(lane, HEAD_SIZE) == sub).astype(F32).astype(BF16)

    def spread(a):
        return jnp.concatenate([a * low, a * high], axis=0)

    ins[0].wait()
    pl.semaphore_wait(barrier, len(peers))

    def rows_of(i, n=BLOCK):
        return pl.ds(i * n, n)

    def x_own(kind, i):
        return send(
            r["tok0"].at[rows_of(i)], r["tok1" if kind == 0 else "tok3"].at[rows_of(i)], "x", kind, (kind, i), at(dx=1 if kind == 0 else 3)
        )

    def x_far(i):
        if i in DIRECT:
            return send(r["tok0"].at[rows_of(i)], r["tok2"].at[rows_of(i)], "x", 2, (2, i), at(dx=2))
        src, dx = ("tok1", 1) if i % 2 == 0 else ("tok3", 3)
        return send(r[src].at[rows_of(i)], r["tok2"].at[rows_of(i)], "x", 2, (2, i), at(dx=dx))

    def z_has(d, k, i):
        return k < 4 or (k == 4 and (i < NB // 2) == (d == 0))

    def z_copy(d, k, i):
        sign = -1 if d == 0 else 1
        src, dst = sign * (k - 1), (4 if k == 4 else sign * k)
        to = at(dz=1 if d == 0 else NZ - 1)
        if k == 4:
            return send(r[f"kv{src}"].at[i], r["kv4"].at[i], "l", d, i, to)
        return send(r[f"kv{src}"].at[i], r[f"kv{dst}"].at[i], "z", (d, k - 1), (d, k - 1, i), to)

    def z_event(k, i):
        for d in (0, 1):
            if z_has(d, k, i):
                z_copy(d, k, i).wait_recv()
                if z_has(d, k + 1, i):
                    z_copy(d, k + 1, i).start()
        if i == NB - 1:
            for dz in (-k, k) if k < 4 else (4,):
                pair(dz).start()

    def pair(dz):
        return send(r[f"kv{dz}"], r[f"other{dz}"], "p", dz + 3, dz + 3, at(flip=True))

    def y_query(j, i):
        return send(r["q0"].at[i], r[f"q{j}"].at[i], "y", j - 1, j - 1, at(dy=j))

    def y_queries(j):
        return send(r["q0"], r[f"q{j}"], "y", j - 1, j - 1, at(dy=j))

    def y_codes(j):
        return send(r["codes0"], r[f"codes{j}"], "c", j - 1, j - 1, at(dy=j))

    def x_wo(j):
        cols = pl.ds(pl.multiple_of(lax.rem(x + j, NX) * PART, PART), PART)
        return send(r["wo"].at[:, cols], r[f"wo{j}"], "w", j - 1, j - 1, at(dx=j))

    def x_gain(j):
        return send(r["gain0"], r[f"gain{j}"], "g", j - 1, j - 1, at(dx=j))

    def y_back(j):
        to = at(dy=NY - j)
        return (
            send(r["po"].at[j - 1], r["ro"].at[j - 1], "b", j - 1, j - 1, to),
            send(r["pm"].at[j - 1], r["rm"].at[j - 1], "m", j - 1, j - 1, to),
        )

    def y_late(j):
        to = at(dy=NY - j)
        return (
            send(r["lo"].at[j - 1], r["eo"].at[j - 1], "e", j - 1, j - 1, to),
            send(r["lm"].at[j - 1], r["em"].at[j - 1], "f", j - 1, j - 1, to),
        )

    def x_att(j, t):
        rows = rows_of(t, 2 * BLOCK)
        return send(r["att0"].at[rows], r[f"att{j}"].at[rows], "a", j - 1, (j - 1, t), at(dx=j))

    sent = []

    def start(copy):
        copy.start()
        sent.append(copy)

    def x_start(i):
        x_own(0, i).start()
        x_own(1, i).start()
        if i in DIRECT:
            x_far(i).start()

    for i in range(AHEAD):
        x_start(i)
    for j in (2, 1, 3):
        y_codes(j).start()
    for copy in ins[1:4]:
        copy.wait()

    def project(i):
        x_far(i).wait_recv()

        def block(_, __):
            total = jnp.zeros((BLOCK, 3 * FEATS), F32)
            for j in range(4):
                part = pl.ds(pl.multiple_of(lax.rem(x + NX - j, NX) * PART, PART), PART)
                total = total + dot(r[f"tok{j}"][rows_of(i), :], r["w"][part, :])
            r["kv0"][i, 0] = total[:, :FEATS].astype(BF16)
            r["kv0"][i, 1] = dot(pick, spread(total[:, FEATS : 2 * FEATS].astype(BF16)), NT).astype(BF16)
            r["q0"][i] = dot(pick, spread(total[:, 2 * FEATS :].astype(BF16)), NT).astype(BF16)

        lax.fori_loop(0, 1, block, None)
        for d in (0, 1):
            z_copy(d, 1, i).start()
        for j in (2, 1, 3):
            y_query(j, i).start()

    for i in range(NB):
        x_own(0, i).wait_recv()
        x_own(1, i).wait_recv()
        if i not in DIRECT:
            x_far(i).start()
        if i + AHEAD < NB:
            x_start(i + AHEAD)
        if i >= 2:
            project(i - 2)
        if i >= 5:
            z_event(1, i - 5)
    project(NB - 2)
    z_event(1, 1)
    project(NB - 1)
    pair(0).start()
    ins[4].wait()
    for j in (2, 1, 3):
        x_wo(j).start()
        x_gain(j).start()
    mine = pl.ds(pl.multiple_of(x * PART, PART), PART)
    r["wo0"][...] = r["wo"][:, mine]
    z_event(1, 2)

    def attend(operands, causal=False):
        scores = [dot(k, spread(q)) * (HEAD_SIZE**-0.5) for q, k, _ in operands]
        if causal:
            visible = sub <= lax.rem(lane, HEAD_SIZE)
            scores = [jnp.where(visible, s, NEG) for s in scores]
        tops = [jnp.max(s, axis=0, keepdims=True) for s in scores]
        weights = [jnp.exp(s - top) for s, top in zip(scores, tops)]
        if causal:
            weights = [jnp.where(visible, w, 0.0) for w in weights]
        masses = [jnp.sum(w, axis=0, keepdims=True) for w in weights]
        blended = [dot(v, spread(w.astype(BF16))) for (_, _, v), w in zip(operands, weights)]
        return list(zip(tops, masses, blended))

    def own(half, _):
        found = attend(
            [(r["q0"][half * 3 + n], r["kv0"][half * 3 + n, 0], r["kv0"][half * 3 + n, 1]) for n in range(3)], causal=True
        )
        for n, (highest, mass, blended) in enumerate(found):
            b = half * 3 + n
            r["own_m"][b, 0:1] = highest
            r["own_m"][b, 1:2] = mass
            r["own_o"][b] = blended

    lax.fori_loop(0, 2, own, None)
    z_event(1, 3)
    for j in (1, 2, 3):
        y_codes(j).wait_recv()
    tables = [pltpu.make_async_copy(r[f"codes{j}"], r["codes_s"].at[j], r["s_codes"].at[j]) for j in range(4)]
    for copy in tables:
        copy.start()
    z_event(1, 4)
    z_event(1, 5)
    for copy in tables:
        copy.wait()
    for j in (1, 2, 3):
        y_queries(j).wait_recv()

    def group(*owners):
        for dz, flip in owners:
            if flip:
                pair(dz).wait_recv()

        def items(_, __):
            operands, places = [], []
            for dz, flip in owners:
                ref = r[f"other{dz}" if flip else f"kv{dz}"]
                side = 1 - c if flip else c
                zz = lax.rem(z + dz + NZ, NZ)
                owner, slot = (zz * NY + y) * 2 + side, zz * 2 + side
                for j in range(4):
                    code = r["codes_s"][j, 0, owner]
                    row, loc = lax.rem(lax.div(code, 8), 8), lax.rem(code, 8)
                    operands.append((r[f"q{j}"][row], ref[loc, 0], ref[loc, 1]))
                    places.append((j, slot, 1 if flip else 0))
            for (j, slot, n), (highest, mass, blended) in zip(places, attend(operands)):
                if owners[0][0] == 4 and j:
                    r["lm"][j - 1, n : n + 1] = highest
                    r["lm"][j - 1, 4 + n : 5 + n] = mass
                    r["lo"][j - 1, n] = blended.astype(BF16)
                else:
                    r["item_m"][j, slot, 0:1] = highest
                    r["item_m"][j, slot, 1:2] = mass
                    r["item_o"][j, slot] = blended

        lax.fori_loop(0, 1, items, None)

    def merged(j, b, mine=False):
        parts = []
        for ch in range(CHOSEN):
            owner = r["codes_s"][j, 1, b * 8 + ch]
            zz = lax.div(owner, 2 * NY)
            ok = jnp.logical_and(lax.rem(lax.div(owner, 2), NY) == y, zz != lax.rem(z + 4, NZ))
            slot = zz * 2 + lax.rem(owner, 2)
            here = jnp.broadcast_to(ok.astype(I32), (1, FEATS)) > 0
            parts.append((here, r["item_m"][j, slot, 0:1], r["item_m"][j, slot, 1:2], r["item_o"][j, slot]))
        if mine:
            yes = jnp.full((1, FEATS), True)
            parts.append((yes, r["own_m"][b, 0:1], r["own_m"][b, 1:2], r["own_o"][b]))
        tops = [jnp.where(here, m, NEG) for here, m, _, _ in parts]
        top = tops[0]
        for m in tops[1:]:
            top = jnp.maximum(top, m)
        mass = jnp.zeros((1, FEATS), F32)
        blended = jnp.zeros((BLOCK, FEATS), F32)
        for (here, _, l, o), m in zip(parts, tops):
            scale = jnp.where(here, jnp.exp(m - top), 0.0)
            mass = mass + scale * l
            blended = blended + scale * o
        return top, mass, blended

    def back(b, j):
        top, mass, blended = merged(j, b)
        t, n = lax.div(b, 2), lax.rem(b, 2)
        r["pm"][j - 1, t, pl.ds(n, 1)] = top
        r["pm"][j - 1, t, pl.ds(4 + n, 1)] = mass
        r["po"][j - 1, b] = blended.astype(BF16)
        return j

    def mine(b, _):
        top, mass, blended = merged(0, b, mine=True)
        r["own_m"][b, 2:3] = top
        r["own_m"][b, 3:4] = mass
        r["own_o"][b] = blended

    groups = [((0, False),), ((0, True),)]
    for k in (1, 2, 3):
        groups += [((-k, False), (k, False)), ((-k, True), (k, True))]
    groups += [((4, False),), ((4, True),)]
    for i in range(NB):
        z_event(2, i)
        if i < 4:
            group(*groups[i])
    for i in range(NB):
        z_event(3, i)
        if i in (1, 3):
            group(*groups[4 + i // 2])
    for i in range(NB):
        z_event(4, i)
        if i in (1, 3):
            group(*groups[6 + i // 2])
        if i == 3:
            for j in (2, 1, 3):
                lax.fori_loop(0, NB, back, j)
                for copy in y_back(j):
                    copy.start()
    lax.fori_loop(0, NB, mine, None)
    group(*groups[8])
    group(*groups[9])
    for j in (2, 1, 3):
        for copy in y_late(j):
            copy.start()
    for j in (1, 2, 3):
        for copy in y_back(j):
            copy.wait_recv()
    for j in (1, 2, 3):
        for copy in y_late(j):
            copy.wait_recv()

    def finish(t, _):
        for n in range(2):
            b = 2 * t + n
            parts = [(r["own_m"][b, 2:3], r["own_m"][b, 3:4], r["own_o"][b])]
            parts += [
                (r["rm"][j, t, n : n + 1], r["rm"][j, t, 4 + n : 5 + n], r["ro"][j, b].astype(F32)) for j in range(3)
            ]
            zz = lax.rem(z + 4, NZ)
            for j in range(4):
                for flip in (0, 1):
                    side = 1 - c if flip else c
                    owner = (zz * NY + lax.rem(y + j, NY)) * 2 + side
                    here = lax.div(r["codes_s"][0, 0, owner], 8) == ASKED // 8 + b
                    here = jnp.broadcast_to(here.astype(I32), (1, FEATS)) > 0
                    if j:
                        part = r["em"][j - 1, flip : flip + 1], r["em"][j - 1, 4 + flip : 5 + flip], r["eo"][j - 1, flip].astype(F32)
                    else:
                        slot = zz * 2 + side
                        part = r["item_m"][0, slot, 0:1], r["item_m"][0, slot, 1:2], r["item_o"][0, slot]
                    parts.append((jnp.where(here, part[0], NEG), jnp.where(here, part[1], 0.0), part[2], here))
            top = parts[0][0]
            for part in parts[1:]:
                top = jnp.maximum(top, part[0])
            mass = jnp.zeros((1, FEATS), F32)
            blended = jnp.zeros((BLOCK, FEATS), F32)
            for m, l, o, *here in parts:
                scale = jnp.exp(m - top)
                if here:
                    scale = jnp.where(here[0], scale, 0.0)
                mass = mass + scale * l
                blended = blended + scale * o
            attended = (blended / mass).astype(BF16)
            r["att0"][rows_of(b), :] = dot(pick, spread(attended), NT).astype(BF16)
        for j in (2, 1, 3):
            x_att(j, t).start()

    lax.fori_loop(0, CH, finish, None)
    for j in (1, 2, 3):
        x_wo(j).wait_recv()
        x_gain(j).wait_recv()

    def close(t, _):
        for j in (1, 2, 3):
            x_att(j, t).wait_recv()
        rows = rows_of(t, 2 * BLOCK)
        wide = [r[f"att{j}"][rows, :].astype(F32) for j in range(4)]
        squares = sum(jnp.sum(a * a, axis=1, keepdims=True) for a in wide)
        scale = lax.rsqrt(squares / (HEADS * HEAD_SIZE) + EPS)
        total = jnp.zeros((2 * BLOCK, PART), F32)
        for j in range(4):
            normed = (wide[j] * scale * r[f"gain{j}"][0:1, :]).astype(BF16)
            total = total + dot(normed, r[f"wo{j}"][...])
        out_ref[rows, :] = total.astype(BF16)

    lax.fori_loop(0, CH, close, None)

    def drain(ref, name, group):
        send(ref, ref, name, group, 0 if name in "lpycwgbmef" else (0, 0, 0) if name == "z" else (0, 0), at(flip=True)).wait_send()

    for kind in range(3):
        drain(r["tok0"], "x", kind)
    for d in (0, 1):
        for k in range(3):
            drain(r["kv0"], "z", (d, k))
        drain(r["kv0"].at[pl.ds(0, NB // 2)], "l", d)
    for dz in range(-3, 5):
        pair(dz).wait_send()
    for j in range(3):
        drain(r["q0"], "y", j)
        drain(r["codes0"], "c", j)
        drain(r["wo0"], "w", j)
        drain(r["gain0"], "g", j)
        drain(r["po"].at[j], "b", j)
        drain(r["pm"].at[j], "m", j)
        drain(r["lo"].at[j], "e", j)
        drain(r["lm"].at[j], "f", j)
        drain(r["att0"], "a", j)


def on_device(tokens, query_weight, key_weight, value_weight, out_weight, norm_gain, chosen_owner, chosen_local):
    hbm = pl.BlockSpec(memory_space=pltpu.HBM)
    vmem = pl.BlockSpec(memory_space=pltpu.VMEM)
    smem = pl.BlockSpec(memory_space=pltpu.SMEM)
    return pl.pallas_call(
        kernel,
        out_shape=jax.ShapeDtypeStruct((NB * BLOCK, PART), BF16),
        in_specs=[hbm] * 5 + [vmem, smem, smem],
        out_specs=vmem,
        scratch_shapes=list(scratch().values()),
        compiler_params=pltpu.CompilerParams(collective_id=0, has_side_effects=True),
        name="attend",
    )(tokens, query_weight, key_weight, value_weight, out_weight, norm_gain.reshape(1, FEATS), chosen_owner, chosen_local)


def solution(mesh):
    return jax.shard_map(
        on_device,
        mesh=mesh,
        in_specs=(
            P("kv", "tp"),
            P(None, "tp"),
            P(None, "tp"),
            P(None, "tp"),
            P("tp", None),
            P("tp"),
            P("kv", None),
            P("kv", None),
        ),
        out_specs=P("kv", "tp"),
        check_vma=False,
    )
```

time: 62.3 us -> 57.3 us (0.920)
  Pallas kernels: 60.5 us -> 55.5 us
    pallas_call x1, Pallas kernels: 60.5 us -> 55.5 us  [on_device(): pl.pallas_call(kernel, out_shape=jax.ShapeDtypeStruct((NB * BLOCK, PART),...]
where the time goes in v3:
time: 57.3 us; the launch traced here: 57.1 us
  Pallas kernels  55.5 us (97%)
  local copies, waits for them, and re-layouts  1.62 us (3%)
    pallas_call x1, Pallas kernels, on_device(): pl.pallas_call(kernel, out_shape=jax.ShapeDtypeStruct((NB * BLOCK, PART),...  55.5 us
    unnamed x1, local copies, waits for them, and re-layouts  1.62 us

profile of v3, /device:TPU:1, one launch (start us, length us, event | category | flops | bytes accessed | tf_op | source)
XLA Modules:
  0.0 57.1 jit_solution(8272565269553051157)
XLA Ops:
  0.0 55.5 %attend.1 = bf16[384,256]{1,0:T(8,128)(2,1)} custom-call(bf16[384,256]{1,0:T(8,128)(2,1)} %tok_hbm.1, bf16[1024,128]{1,0:T(8,128)(2,1)} %wq_hbm.1, bf16[1024,128]{1,0:T(8,128)(2,1)} %wk_hbm.1, bf16[1024,128]{1,0:T(8,128)(2,1)} %wv_hbm.1, bf16[128,1024]{1,0:T(8,128)(2,1)} %wo_hbm.1, f32[1,128]{1,0:T(1,128)} %bitcast.1, s32[6,8]{1,0:T(8,128)} %owner_ref.1, ...), custom_call_target="tpu_custom_call" | custom-call | tf_op jit(solution)/shard_map/attend/pallas_call | solution.py:490
  55.5 1.6 %copy.10 = bf16[384,256]{1,0:T(8,128)(2,1)} copy(bf16[384,256]{1,0:T(8,128)(2,1)} %attend.1) | data formatting | bytes 393216
